TPU v7x, 512 devices: a whole 4x8x8 slice. The times are simulated.
512 devices in a mesh: sp: 256 (over z, y, x), tp: 2 (over core).
Axes of the slice: x: 4, y: 8, z: 8, core: 2. Of those that a mesh axis runs over, the one named last changes fastest.
Arguments:
- tokens: bfloat16 [131072, 2048], P(('sp', 'tp')), may hold values from -6 to 6
- norm_gain: float32 [2048], replicated, may hold values from 0.1 to 1.9
- in_weight: bfloat16 [2048, 1024], P(None, 'tp'), may hold values from -0.125 to 0.125
- gate_weight: bfloat16 [2048, 1024], P(None, 'tp'), may hold values from -0.125 to 0.125
- conv_weight: float32 [4, 1024], P(None, 'tp'), may hold values from -3 to 3
- decay_gate_weight: bfloat16 [16, 64, 64], P('tp'), may hold values from -0.75 to 0.75
- decay_gate_bias: float32 [1024], P('tp'), may hold values from -4 to 4
- input_gate_weight: bfloat16 [16, 64, 64], P('tp'), may hold values from -0.75 to 0.75
- input_gate_bias: float32 [1024], P('tp'), may hold values from -4 to 4
- channel_decay_rate: float32 [1024], P('tp'), may hold values from 3.0517578e-07 to 0.01
- forgetting_offset: float32 [16, 131072], P('tp', 'sp'), may hold values from -1.6 to 0
- out_weight: bfloat16 [1024, 2048], P('tp'), may hold values from -0.1875 to 0.1875
Outputs:
- mixed: bfloat16 [131072, 2048], P(('sp', 'tp'))
All inputs are finite; a program needn't handle non-finite values.
Results may differ from a plain program's by a relative error of at most 0.0067.
Values may be sent and summed in bfloat16 or wider, within the bound.
No kernel may reach another device: no remote copies, remote signals or barrier semaphores. Data moves between devices by JAX's collectives and lax.ppermute only.
A program may use at most 64 MiB of HBM per device.

v0:
```python
import jax
import jax.numpy as jnp
from jax import lax
from jax.experimental import pallas as pl
from jax.experimental.pallas import tpu as pltpu
from jax.sharding import Mesh
from jax.sharding import PartitionSpec as P

SP = ("sp_0", "sp_1", "sp_2")
PLANE = ("sp_1", "sp_2")
SP_TP = ("sp_0", "sp_1", "sp_2", "tp")

EPSILON = 1e-05
SUB = 8
HALO = 8
f32, bf16 = jnp.float32, jnp.bfloat16


def dot(a, b):
    return jnp.dot(a, b, preferred_element_type=f32)


def normalized(x, gain):
    x = x.astype(f32)
    centered = x - jnp.mean(x, axis=1, keepdims=True)
    spread = jnp.mean(centered * centered, axis=1, keepdims=True)
    return centered * lax.rsqrt(spread + EPSILON) * gain


def sigmoid(x):
    return 1.0 / (1.0 + jnp.exp(-x))


def local_kernel(other, halo_a, halo_b, *refs):
    stored, refs = refs[:ARGS], refs[ARGS:]
    h_out, p_out, g_out, runs_out, sent_out, *refs = refs
    gain, own, conv, w_decay, b_decay, w_input, b_input, rate, offset, *refs = refs
    w_in, w_gate, arrived, normed, middle, scale, smoothed, pre_r, pre_i, shift, blocks, extended = refs
    half, width = own.shape[0], w_in.shape[1]
    held = (gain, w_in, own, w_gate, conv, w_decay, b_decay, w_input, b_input, rate, offset)
    copies = [pltpu.make_async_copy(a, b, arrived.at[i]) for i, (a, b) in enumerate(zip(stored, held))]
    length = 2 * half
    run = length // SUB
    taps = conv.shape[0]
    lead = (taps - 1) * SUB
    tp = lax.axis_index("tp")
    step, lanes = 32, 128
    features = own.shape[1]

    def tiles(source, r):
        return [source[r, t : t + lanes].astype(f32) for t in range(0, features, lanes)]

    def by_rows(one):
        def rows(i, _):
            one(pl.multiple_of(i * step, step))
            return 0

        lax.fori_loop(0, half // step, rows, 0)

    def over_features(stat):
        return jnp.broadcast_to(jnp.sum(stat[...], axis=1, keepdims=True) * (1.0 / features), stat.shape)

    def norm_tokens(source, base, ready=None):
        def add_up(i):
            r = pl.ds(i, step)
            middle[r, :] = sum(tiles(source, r))

        by_rows(add_up)
        middle[...] = over_features(middle)

        def add_squares(i):
            r = pl.ds(i, step)
            m = middle[r, :]
            scale[r, :] = sum((x - m) * (x - m) for x in tiles(source, r))

        by_rows(add_squares)
        scale[...] = lax.rsqrt(over_features(scale) + EPSILON)
        if ready is not None:
            ready.wait()

        def write(i):
            r = pl.ds(i, step)
            m, k = middle[r, :], scale[r, :]
            d = pl.ds(pl.multiple_of(base + i, step), step)
            for t, x in zip(range(0, features, lanes), tiles(source, r)):
                normed[d, t : t + lanes] = ((x - m) * k * gain[:, t : t + lanes]).astype(bf16)

        by_rows(write)

    for i in (0, 2, 1, *range(3, ARGS)):
        copies[i].start()
    norm_tokens(other, (1 - tp) * half, copies[0])
    halo = normalized(jnp.where(tp == 1, halo_a[...].astype(f32), halo_b[...].astype(f32)), gain[...])
    normed[pl.ds(length, 2 * HALO), :] = jnp.concatenate([halo, jnp.zeros_like(halo)], axis=0).astype(bf16)
    copies[2].wait()
    norm_tokens(own, tp * half)
    copies[1].wait()
    both = dot(normed[...], w_in[...]).astype(bf16)
    inner, inner_before = both[:length], both[length:]
    for copy in copies[3:]:
        copy.wait()
    gate = dot(normed[:length, :], w_gate[...]).astype(bf16)

    def picks(rows, base):
        r = lax.broadcasted_iota(jnp.int32, (rows, length), 0)
        c = lax.broadcasted_iota(jnp.int32, (rows, length), 1)
        return jnp.where(c == (r & (SUB - 1)) * run + (r >> 3) + base, 1.0, 0.0).astype(bf16)

    order = picks(length, 0)
    extended[pl.ds(lead, length), :] = dot(order, inner)
    r = lax.broadcasted_iota(jnp.int32, (lead, 2 * HALO), 0)
    c = lax.broadcasted_iota(jnp.int32, (lead, 2 * HALO), 1)
    from_halo = jnp.where(((r & (SUB - 1)) == 0) & (c == (r >> 3) + HALO - taps + 1), 1.0, 0.0).astype(bf16)
    extended[pl.ds(0, lead), :] = dot(picks(lead, 1 - taps), inner) + dot(from_halo, inner_before)
    g_out[...] = jax.nn.gelu(dot(order, gate))

    smooth = extended[pl.ds(0, length), :] * conv[0:1, :]
    for tap in range(1, taps):
        smooth = smooth + extended[pl.ds(tap * SUB, length), :] * conv[tap : tap + 1, :]
    smoothed[...] = smooth.astype(bf16)

    heads, block = w_decay.shape[0], w_decay.shape[1]
    wide = 256
    per = wide // block
    blocks[...] = jnp.zeros_like(blocks)
    for head in range(heads):
        q, i = head // per, (head % per) * block
        blocks[q, pl.ds(i, block), pl.ds(i, block)] = w_decay[head]
        blocks[q, pl.ds(i, block), pl.ds(wide + i, block)] = w_input[head]
    for q in range(heads // per):
        both = dot(smoothed[:, q * wide : (q + 1) * wide], blocks[q])
        pre_r[:, q * wide : (q + 1) * wide] = both[:, :wide]
        pre_i[:, q * wide : (q + 1) * wide] = both[:, wide:]

    part0 = offset[...].astype(bf16).astype(f32)
    part1 = (offset[...] - part0).astype(bf16).astype(f32)
    part2 = offset[...] - part0 - part1
    parts = jnp.concatenate([part0, part1, part2, jnp.zeros_like(part0)], axis=0).astype(bf16)
    moved = lax.dot_general(parts, order, (((1,), (1,)), ((), ())), preferred_element_type=f32).astype(bf16)
    r = lax.broadcasted_iota(jnp.int32, (4 * heads, width), 0)
    c = lax.broadcasted_iota(jnp.int32, (4 * heads, width), 1)
    spread = jnp.where((r & (heads - 1)) == (c >> 6), -1.0, 0.0).astype(bf16)
    shift[...] = lax.dot_general(moved, spread, (((0,), (0,)), ((), ())), preferred_element_type=f32)

    rows = 4 * SUB

    def scan_rows(i, carry):
        h, p = carry
        at = pl.ds(pl.multiple_of(i * rows, rows), rows)
        retain = sigmoid(pre_r[at, :] + b_decay[...])
        admit = sigmoid(pre_i[at, :] + b_input[...])
        loss = retain * (8.0 * rate[...]) + shift[at, :]
        decay = jnp.exp(-loss)
        rest = jnp.tanh(loss) * (1.0 + decay * decay)
        drive = rest * lax.rsqrt(jnp.maximum(rest, 1e-37)) * admit * smoothed[at, :].astype(f32)
        for k in range(rows // SUB):
            a = decay[k * SUB : (k + 1) * SUB, :]
            h = a * h + drive[k * SUB : (k + 1) * SUB, :]
            p = a * p
            here = pl.ds(pl.multiple_of(i * rows + k * SUB, SUB), SUB)
            h_out[here, :] = h
            p_out[here, :] = p
        return h, p

    h, p = lax.fori_loop(
        0, length // rows, scan_rows, (jnp.zeros((SUB, width), f32), jnp.ones((SUB, width), f32))
    )
    a_before, b_before = jnp.ones((1, width), f32), jnp.zeros((1, width), f32)
    for s in range(SUB):
        runs_out[0, s : s + 1, :] = a_before
        runs_out[1, s : s + 1, :] = b_before
        a_before, b_before = a_before * p[s : s + 1, :], p[s : s + 1, :] * b_before + h[s : s + 1, :]
    pair = jnp.concatenate([a_before, b_before], axis=0)
    sent_out[...] = jnp.broadcast_to(pair[None], sent_out.shape)


def before_in(pieces, index):
    width = pieces.shape[2]
    a, b = jnp.ones((1, width), f32), jnp.zeros((1, width), f32)
    a_at, b_at = a, b
    for k in range(pieces.shape[0]):
        here = k == index
        a_at, b_at = jnp.where(here, a, a_at), jnp.where(here, b, b_at)
        a_k, b_k = pieces[k, 0:1, :], pieces[k, 1:2, :]
        a, b = a * a_k, a_k * b + b_k
    return (a_at, b_at), (a, b)


def plane_kernel(pieces, before_out, sent_out):
    index = lax.axis_index("sp_1") * lax.axis_size("sp_2") + lax.axis_index("sp_2")
    (a_at, b_at), (a, b) = before_in(pieces, index)
    before_out[...] = jnp.concatenate([a_at, b_at], axis=0)
    pair = jnp.concatenate([a, b], axis=0)
    sent_out[...] = jnp.broadcast_to(pair[None], sent_out.shape)


def state_kernel(pieces, before, runs, h, p, g, mine_out, theirs_out, gated):
    (_, b_at), _ = before_in(pieces, lax.axis_index("sp_0"))
    carried = before[0:1, :] * b_at + before[1:2, :]
    start = runs[0] * carried + runs[1]
    length = h.shape[0]
    half, run = length // 2, length // SUB
    rows = 4 * SUB
    starts = jnp.concatenate([start] * (rows // SUB), axis=0)

    def state_rows(i, _):
        at = pl.ds(pl.multiple_of(i * rows, rows), rows)
        gated[at, :] = ((h[at, :] + p[at, :] * starts) * g[at, :]).astype(bf16)
        return 0

    lax.fori_loop(0, length // rows, state_rows, 0, unroll=2)
    tp = lax.axis_index("tp")

    def back(first):
        t = lax.broadcasted_iota(jnp.int32, (half, length), 0) + first
        c = lax.broadcasted_iota(jnp.int32, (half, length), 1)
        pick = jnp.where(t == (c & (SUB - 1)) * run + (c >> 3), 1.0, 0.0).astype(bf16)
        return dot(pick, gated[...]).astype(bf16)

    theirs_out[...] = back((1 - tp) * half)
    mine_out[...] = back(tp * half)


def out_kernel(mine, theirs, w_mine, w_theirs, out, block, sent):
    cols = block.shape[2]
    copies = []
    for i in range(block.shape[0]):
        at = pl.ds(i * cols, cols)
        block[i] = (dot(mine[...], w_mine[:, at]) + dot(theirs[...], w_theirs[:, at])).astype(bf16)
        copies.append(pltpu.make_async_copy(block.at[i], out.at[:, at], sent.at[i]))
        copies[i].start()
    for copy in copies:
        copy.wait()


VMEM = pl.BlockSpec(memory_space=pltpu.VMEM)


HBM = pl.BlockSpec(memory_space=pltpu.HBM)
ARGS = 11


def call(kernel, inputs, out_shape, scratch=(), out_specs=None):
    run = pl.pallas_call(
        kernel,
        out_shape=out_shape,
        out_specs=out_specs or jax.tree.map(lambda _: VMEM, out_shape),
        scratch_shapes=list(scratch),
        compiler_params=pltpu.CompilerParams(vmem_limit_bytes=32 * 1024 * 1024),
        in_specs=[VMEM] * inputs[0] + [HBM] * inputs[1],
    )

    def place(i, a):
        return pltpu.with_memory_space_constraint(a, pltpu.VMEM if i < inputs[0] else pltpu.HBM)

    return lambda *args: run(*(place(i, a) for i, a in enumerate(args)))


def step(
    tokens,
    norm_gain,
    in_weight,
    gate_weight,
    conv_weight,
    decay_gate_weight,
    decay_gate_bias,
    input_gate_weight,
    input_gate_bias,
    channel_decay_rate,
    forgetting_offset,
    out_weight,
):
    half, features = tokens.shape
    length = 2 * half
    width = in_weight.shape[1]
    heads, block = decay_gate_weight.shape[:2]
    count = lax.axis_size(SP)
    plane = lax.axis_size(PLANE)
    deep = lax.axis_size("sp_0")
    S = jax.ShapeDtypeStruct

    swap = [(0, 1), (1, 0)]
    tail = tokens[half - HALO :]
    halo_a = lax.ppermute(tail, SP_TP, [(2 * s + 1, 2 * s + 3) for s in range(count - 1)])
    halo_b = lax.ppermute(tail, SP_TP, [(2 * s + 1, 2 * s + 2) for s in range(count - 1)])
    other = lax.ppermute(tokens, "tp", swap)
    w_theirs = lax.ppermute(out_weight, "tp", swap)

    row = lambda v: v.reshape(1, -1)
    fetched = (
        row(norm_gain), in_weight, tokens, gate_weight,
        conv_weight, decay_gate_weight, row(decay_gate_bias),
        input_gate_weight, row(input_gate_bias), row(channel_decay_rate), forgetting_offset,
    )
    big = pltpu.VMEM
    h, p, g, runs, sent = call(
        local_kernel,
        (3, ARGS),
        (
            big((length, width), f32),
            big((length, width), f32),
            big((length, width), f32),
            big((2, SUB, width), f32),
            big((plane, 2, width), f32),
        ),
        scratch=[big(a.shape, a.dtype) for i, a in enumerate(fetched) if i not in (1, 3)]
        + [
            big((features, width), bf16),
            big((features, width), bf16),
            pltpu.SemaphoreType.DMA((ARGS,)),
            big((length + 2 * HALO, features), bf16),
            big((half, 128), f32),
            big((half, 128), f32),
            big((length, width), bf16),
            big((length, width), f32),
            big((length, width), f32),
            big((length, width), f32),
            big((heads * block // 256, 256, 512), bf16),
            big((length + (conv_weight.shape[0] - 1) * SUB, width), f32),
        ],
    )(other, halo_a, halo_b, *fetched)
    pieces = lax.all_to_all(sent, PLANE, split_axis=0, concat_axis=0, tiled=True)
    before, sent = call(plane_kernel, (1, 0), (big((2, width), f32), big((deep, 2, width), f32)))(pieces)
    pieces = lax.all_to_all(sent, "sp_0", split_axis=0, concat_axis=0, tiled=True)
    mine, theirs = call(
        state_kernel,
        (6, 0),
        (big((half, width), bf16), big((half, width), bf16)),
        scratch=(big((length, width), bf16),),
    )(pieces, before, runs, h, p, g)
    received = lax.ppermute(theirs, "tp", swap)
    cols = 512
    return call(
        out_kernel,
        (4, 0),
        S((half, features), bf16),
        scratch=(big((features // cols, half, cols), bf16), pltpu.SemaphoreType.DMA((features // cols,))),
        out_specs=HBM,
    )(mine, received, out_weight, w_theirs)


def solution(mesh):
    torus = Mesh(mesh.devices.reshape(8, 8, 4, mesh.shape["tp"]), SP_TP)
    placed = (
        P(SP_TP, None),
        P(),
        P(None, "tp"),
        P(None, "tp"),
        P(None, "tp"),
        P("tp", None, None),
        P("tp"),
        P("tp", None, None),
        P("tp"),
        P("tp"),
        P("tp", SP),
        P("tp", None),
    )
    return jax.shard_map(step, mesh=torus, in_specs=placed, out_specs=P(SP_TP, None), check_vma=False)
```

profile of v0, /device:TPU:1, one launch (start us, length us, event | category | flops | bytes accessed | tf_op | source)
XLA Modules:
  0.0 66.2 jit_solution(7425337505203383420)
XLA Ops:
  0.0 8.7 %collective-permute-start.4 = (bf16[512,2048]{1,0:T(8,128)(2,1)}, bf16[512,2048]{1,0:T(8,128)(2,1)S(1)}, u32[]{:S(2)}, u32[]{:S(2)}) collective-permute-start(bf16[512,2048]{1,0:T(8,128)(2,1)} %w_mine.1), channel_id=1, source_target_pairs={{0,1},{1,0},{2,3},{3,2},{4,5},{5,4},{6,7},{7,6},{8,9},{9,8},{10,11... | collective-permute-start | bytes 6291464 | tf_op jit(solution)/shard_map/ppermute | solution.py:287
  8.7 1.9 %collective-permute-start = (bf16[256,2048]{1,0:T(8,128)(2,1)}, bf16[256,2048]{1,0:T(8,128)(2,1)S(1)}, u32[]{:S(2)}, u32[]{:S(2)}) collective-permute-start(bf16[256,2048]{1,0:T(8,128)(2,1)} %refs_2_.1), channel_id=1, source_target_pairs={{0,1},{1,0},{2,3},{3,2},{4,5},{5,4},{6,7},{7,6},{8,9},{9,8},{10,11... | collective-permute-start | bytes 3145736 | tf_op jit(solution)/shard_map/ppermute | solution.py:286
  10.7 0.8 %slice.3 = bf16[8,2048]{1,0:T(8,128)(2,1)S(1)} slice(bf16[256,2048]{1,0:T(8,128)(2,1)} %refs_2_.1), slice={[248:256], [0:2048]} | slice | bytes 65536 | tf_op jit(solution)/shard_map/slice | solution.py:283
  11.4 1.3 %collective-permute-start.1 = (bf16[8,2048]{1,0:T(8,128)(2,1)S(1)}, bf16[8,2048]{1,0:T(8,128)(2,1)S(1)}, u32[]{:S(2)}, u32[]{:S(2)}) collective-permute-start(bf16[8,2048]{1,0:T(8,128)(2,1)S(1)} %slice.3), channel_id=1, source_target_pairs={{1,3},{3,5},{5,7},{7,9},{9,11},{11,13},{13,15},{15,17},{17,19},{19... | collective-permute-start | bytes 98312 | tf_op jit(solution)/shard_map/ppermute | solution.py:284
  12.7 1.3 %collective-permute-start.2 = (bf16[8,2048]{1,0:T(8,128)(2,1)S(1)}, bf16[8,2048]{1,0:T(8,128)(2,1)S(1)}, u32[]{:S(2)}, u32[]{:S(2)}) collective-permute-start(bf16[8,2048]{1,0:T(8,128)(2,1)S(1)} %slice.3), channel_id=1, source_target_pairs={{1,2},{3,4},{5,6},{7,8},{9,10},{11,12},{13,14},{15,16},{17,18},{19... | collective-permute-start | bytes 98312 | tf_op jit(solution)/shard_map/ppermute | solution.py:285
  14.0 0.0 collective-permute-done.1.halo_a
  14.0 1.0 %collective-permute-done.2.halo_b = bf16[8,2048]{1,0:T(8,128)(2,1)S(1)} collective-permute-done((bf16[8,2048]{1,0:T(8,128)(2,1)S(1)}, bf16[8,2048]{1,0:T(8,128)(2,1)S(1)}, u32[]{:S(2)}, u32[]{:S(2)}) %collective-permute-start.2) | collective-permute-done | bytes 32800 | tf_op jit(solution)/shard_map/ppermute | solution.py:285
  15.0 0.0 collective-permute-done.other
  15.0 8.2 %shard_map.118 = (f32[512,512]{1,0:T(8,128)S(1)}, f32[512,512]{1,0:T(8,128)S(1)}, f32[512,512]{1,0:T(8,128)S(1)}, f32[2,8,512]{2,1,0:T(8,128)S(1)}, f32[32,2,512]{2,1,0:T(2,128)S(1)}) custom-call(bf16[256,2048]{1,0:T(8,128)(2,1)S(1)} %collective-permute-done.other, bf16[8,2048]{1,0:T(8,128)(2,1)S(1)} %collective-permute-done.1.halo_a, ...), custom_call_target="tpu_custom_call" | custom-call | tf_op jit(solution)/shard_map/pallas_call | solution.py:256
  23.3 0.0 copy-start
  23.3 15.6 %all_to_all.10.pieces = f32[32,2,512]{2,1,0:T(2,128)S(1)} all-to-all(f32[32,2,512]{2,1,0:T(2,128)S(1)} %get-tuple-element.14), channel_id=1, replica_groups=mesh['sp_0'=8,'sp_1'=8,'sp_2'=4,'tp'=2] {'sp_1','sp_2'}, dimensions={0} | all-to-all | bytes 262144 | tf_op jit(solution)/shard_map/all_to_all | solution.py:322
  38.9 0.1 shard_map.119
  39.0 16.7 %all_to_all.11.pieces = f32[8,2,512]{2,1,0:T(2,128)S(1)} all-to-all(f32[8,2,512]{2,1,0:T(2,128)S(1)} %get-tuple-element.15), channel_id=1, replica_groups=mesh['sp_0'=8,'sp_1'=8,'sp_2'=4,'tp'=2] {'sp_0'}, dimensions={0} | all-to-all | bytes 65536 | tf_op jit(solution)/shard_map/all_to_all | solution.py:324
  55.7 0.6 shard_map.120
  56.4 6.7 %collective-permute-start.3 = (bf16[256,512]{1,0:T(8,128)(2,1)S(1)}, bf16[256,512]{1,0:T(8,128)(2,1)S(1)}, u32[]{:S(2)}, u32[]{:S(2)}) collective-permute-start(bf16[256,512]{1,0:T(8,128)(2,1)S(1)} %get-tuple-element.22), channel_id=1, source_target_pairs={{0,1},{1,0},{2,3},{3,2},{4,5},{5,4},{6,7},{7,6},{8,9},{9,8},{10,11... | collective-permute-start | bytes 786440 | tf_op jit(solution)/shard_map/ppermute | solution.py:331
  63.1 1.1 %collective-permute-done.3.theirs = bf16[256,512]{1,0:T(8,128)(2,1)S(1)} collective-permute-done((bf16[256,512]{1,0:T(8,128)(2,1)S(1)}, bf16[256,512]{1,0:T(8,128)(2,1)S(1)}, u32[]{:S(2)}, u32[]{:S(2)}) %collective-permute-start.3) | collective-permute-done | bytes 262176 | tf_op jit(solution)/shard_map/ppermute | solution.py:331
  64.2 0.0 collective-permute-done.4.w_theirs
  64.2 0.0 copy-done
  64.2 2.0 %shard_map.121 = bf16[256,2048]{1,0:T(8,128)(2,1)} custom-call(bf16[256,512]{1,0:T(8,128)(2,1)S(1)} %get-tuple-element.21.mine, bf16[256,512]{1,0:T(8,128)(2,1)S(1)} %collective-permute-done.3.theirs, bf16[512,2048]{1,0:T(8,128)(2,1)S(1)} %copy-done, bf16[512,2048]{1,0:T(8,128)(2,1)S(1)} %collective-permute-done.4.w_theirs), custom_call_target="tpu_custom_call" | custom-call | tf_op jit(solution)/shard_map/pallas_call | solution.py:256
Async XLA Ops:
  0.0 64.2 %collective-permute-start.4 = (bf16[512,2048]{1,0:T(8,128)(2,1)}, bf16[512,2048]{1,0:T(8,128)(2,1)S(1)}, u32[]{:S(2)}, u32[]{:S(2)}) collective-permute-start(bf16[512,2048]{1,0:T(8,128)(2,1)} %w_mine.1), channel_id=1, source_target_pairs={{0,1},{1,0},{2,3},{3,2},{4,5},{5,4},{6,7},{7,6},{8,9},{9,8},{10,11... | collective-permute-start | bytes 6291464 | tf_op jit(solution)/shard_map/ppermute | solution.py:287
  8.7 6.3 %collective-permute-start = (bf16[256,2048]{1,0:T(8,128)(2,1)}, bf16[256,2048]{1,0:T(8,128)(2,1)S(1)}, u32[]{:S(2)}, u32[]{:S(2)}) collective-permute-start(bf16[256,2048]{1,0:T(8,128)(2,1)} %refs_2_.1), channel_id=1, source_target_pairs={{0,1},{1,0},{2,3},{3,2},{4,5},{5,4},{6,7},{7,6},{8,9},{9,8},{10,11... | collective-permute-start | bytes 3145736 | tf_op jit(solution)/shard_map/ppermute | solution.py:286
  11.4 2.6 %collective-permute-start.1 = (bf16[8,2048]{1,0:T(8,128)(2,1)S(1)}, bf16[8,2048]{1,0:T(8,128)(2,1)S(1)}, u32[]{:S(2)}, u32[]{:S(2)}) collective-permute-start(bf16[8,2048]{1,0:T(8,128)(2,1)S(1)} %slice.3), channel_id=1, source_target_pairs={{1,3},{3,5},{5,7},{7,9},{9,11},{11,13},{13,15},{15,17},{17,19},{19... | collective-permute-start | bytes 98312 | tf_op jit(solution)/shard_map/ppermute | solution.py:284
  12.7 2.3 %collective-permute-start.2 = (bf16[8,2048]{1,0:T(8,128)(2,1)S(1)}, bf16[8,2048]{1,0:T(8,128)(2,1)S(1)}, u32[]{:S(2)}, u32[]{:S(2)}) collective-permute-start(bf16[8,2048]{1,0:T(8,128)(2,1)S(1)} %slice.3), channel_id=1, source_target_pairs={{1,2},{3,4},{5,6},{7,8},{9,10},{11,12},{13,14},{15,16},{17,18},{19... | collective-permute-start | bytes 98312 | tf_op jit(solution)/shard_map/ppermute | solution.py:285
  23.3 40.9 %copy-start = (bf16[512,2048]{1,0:T(8,128)(2,1)S(1)}, bf16[512,2048]{1,0:T(8,128)(2,1)}, u32[]{:S(2)}) copy-start(bf16[512,2048]{1,0:T(8,128)(2,1)} %w_mine.1) | copy-start | bytes 6291460
  56.4 7.8 %collective-permute-start.3 = (bf16[256,512]{1,0:T(8,128)(2,1)S(1)}, bf16[256,512]{1,0:T(8,128)(2,1)S(1)}, u32[]{:S(2)}, u32[]{:S(2)}) collective-permute-start(bf16[256,512]{1,0:T(8,128)(2,1)S(1)} %get-tuple-element.22), channel_id=1, source_target_pairs={{0,1},{1,0},{2,3},{3,2},{4,5},{5,4},{6,7},{7,6},{8,9},{9,8},{10,11... | collective-permute-start | bytes 786440 | tf_op jit(solution)/shard_map/ppermute | solution.py:331
where the time goes:
time: 66.6 us; the launch traced here: 66.2 us
  blocking collectives  32.3 us (48%)
  starting transfers between devices  19.9 us (30%)
  Pallas kernels  11 us (17%)
  waiting for transfers between devices  2.14 us (3%)
  local copies, waits for them, and re-layouts  0.77 us (1%)
    all_to_all x1, blocking collectives, step(): lax.all_to_all(sent, 'sp_0', split_axis=0, concat_axis=0, tiled=True)  16.7 us
    all_to_all x1, blocking collectives, step(): lax.all_to_all(sent, PLANE, split_axis=0, concat_axis=0, tiled=True)  15.6 us
    pallas_call x4, Pallas kernels, call(): return lambda *args: run(*(place(i, a) for i, a in enumerate(args)))  11 us
    ppermute x1, starting transfers between devices, step(): w_theirs = lax.ppermute(out_weight, 'tp', swap)  8.74 us
    ppermute x1, starting transfers between devices, step(): received = lax.ppermute(theirs, 'tp', swap)  6.7 us
    ppermute x1, starting transfers between devices, step(): other = lax.ppermute(tokens, 'tp', swap)  1.92 us
  transfers between devices with their start and end apart: 5, of which 2 were waited for; matrix products, arithmetic and copies ran while one was open for 1% of the time, Pallas kernels for 14%

commit v1 on v0

v1 whole, which is shorter than its diff:
```python
import jax
import jax.numpy as jnp
from jax import lax
from jax.experimental import pallas as pl
from jax.experimental.pallas import tpu as pltpu
from jax.sharding import Mesh
from jax.sharding import PartitionSpec as P

SP = ("sp_0", "sp_1", "sp_2")
PLANE = ("sp_1", "sp_2")
SP_TP = ("sp_0", "sp_1", "sp_2", "tp")

EPSILON = 1e-05
SUB = 8
HALO = 8
f32, bf16 = jnp.float32, jnp.bfloat16


def dot(a, b):
    return jnp.dot(a, b, preferred_element_type=f32)


def sigmoid(x):
    return 1.0 / (1.0 + jnp.exp(-x))


def project_kernel(other, *refs):
    stored, refs = refs[:ARGS], refs[ARGS:]
    inner, tail, normed, *held = refs[: ARGS]
    gain, w_in, own, arrived, middle, scale = refs[ARGS:]
    held = (gain, w_in, own, *held)
    copies = [pltpu.make_async_copy(a, b, arrived.at[i]) for i, (a, b) in enumerate(zip(stored, held))]
    half, features = own.shape
    tp = lax.axis_index("tp")
    step, lanes = 32, 128

    def tiles(source, r):
        return [source[r, t : t + lanes].astype(f32) for t in range(0, features, lanes)]

    def by_rows(one):
        def rows(i, _):
            one(pl.multiple_of(i * step, step))
            return 0

        lax.fori_loop(0, half // step, rows, 0)

    def over_features(stat):
        return jnp.broadcast_to(jnp.sum(stat[...], axis=1, keepdims=True) * (1.0 / features), stat.shape)

    def norm_tokens(source, base, ready=None):
        def add_up(i):
            r = pl.ds(i, step)
            middle[r, :] = sum(tiles(source, r))

        by_rows(add_up)
        middle[...] = over_features(middle)

        def add_squares(i):
            r = pl.ds(i, step)
            m = middle[r, :]
            scale[r, :] = sum((x - m) * (x - m) for x in tiles(source, r))

        by_rows(add_squares)
        scale[...] = lax.rsqrt(over_features(scale) + EPSILON)
        if ready is not None:
            ready.wait()

        def write(i):
            r = pl.ds(i, step)
            m, k = middle[r, :], scale[r, :]
            d = pl.ds(pl.multiple_of(base + i, step), step)
            for t, x in zip(range(0, features, lanes), tiles(source, r)):
                normed[d, t : t + lanes] = ((x - m) * k * gain[:, t : t + lanes]).astype(bf16)

        by_rows(write)

    for i in (0, 2, 1, *range(3, ARGS)):
        copies[i].start()
    norm_tokens(other, (1 - tp) * half, copies[0])
    copies[2].wait()
    norm_tokens(own, tp * half)
    copies[1].wait()
    both = dot(normed[...], w_in[...]).astype(bf16)
    inner[...] = both
    tail[...] = both[2 * half - HALO :]
    for copy in copies[3:]:
        copy.wait()


def gates(pre_r, pre_i, x, b_decay, b_input, rate, shift):
    retain = sigmoid(pre_r + b_decay)
    admit = sigmoid(pre_i + b_input)
    loss = retain * (8.0 * rate) + shift
    decay = jnp.exp(-loss)
    rest = jnp.tanh(loss) * (1.0 + decay * decay)
    return decay, rest * lax.rsqrt(jnp.maximum(rest, 1e-37)) * admit * x


def block_dots(smoothed, blocks, store):
    wide = blocks.shape[1]
    for q in range(blocks.shape[0]):
        at = slice(q * wide, (q + 1) * wide)
        both = dot(smoothed[:, at], blocks[q])
        store(at, both[:, :wide], both[:, wide:])


def scan_kernel(
    inner, normed, w_gate, conv, w_decay, b_decay, w_input, b_input, rate, offset,
    h_out, p_out, g_out, ends_out, blocks, heads_shift,
    smoothed, pre_r, pre_i, shift, extended,
):
    length, width = inner.shape
    run = length // SUB
    taps = conv.shape[0]
    lead = (taps - 1) * SUB

    def picks(rows, base):
        r = lax.broadcasted_iota(jnp.int32, (rows, length), 0)
        c = lax.broadcasted_iota(jnp.int32, (rows, length), 1)
        return jnp.where(c == (r & (SUB - 1)) * run + (r >> 3) + base, 1.0, 0.0).astype(bf16)

    order = picks(length, 0)
    extended[pl.ds(lead, length), :] = dot(order, inner[...])
    extended[pl.ds(0, lead), :] = dot(picks(lead, 1 - taps), inner[...])
    gate = dot(normed[...], w_gate[...]).astype(bf16)
    g_out[...] = jax.nn.gelu(dot(order, gate))

    smooth = extended[pl.ds(0, length), :] * conv[0:1, :]
    for tap in range(1, taps):
        smooth = smooth + extended[pl.ds(tap * SUB, length), :] * conv[tap : tap + 1, :]
    smoothed[...] = smooth.astype(bf16)

    heads, block = w_decay.shape[0], w_decay.shape[1]
    wide = blocks.shape[1]
    per = wide // block
    blocks[...] = jnp.zeros_like(blocks)
    for head in range(heads):
        q, i = head // per, (head % per) * block
        blocks[q, pl.ds(i, block), pl.ds(i, block)] = w_decay[head]
        blocks[q, pl.ds(i, block), pl.ds(wide + i, block)] = w_input[head]

    def store(at, r, i):
        pre_r[:, at] = r
        pre_i[:, at] = i

    block_dots(smoothed, blocks, store)

    part0 = offset[...].astype(bf16).astype(f32)
    part1 = (offset[...] - part0).astype(bf16).astype(f32)
    part2 = offset[...] - part0 - part1
    parts = jnp.concatenate([part0, part1, part2, jnp.zeros_like(part0)], axis=0).astype(bf16)
    moved = lax.dot_general(parts, order, (((1,), (1,)), ((), ())), preferred_element_type=f32).astype(bf16)
    r = lax.broadcasted_iota(jnp.int32, (4 * heads, width), 0)
    c = lax.broadcasted_iota(jnp.int32, (4 * heads, width), 1)
    spread = jnp.where((r & (heads - 1)) == (c >> 6), -1.0, 0.0).astype(bf16)
    shift[...] = lax.dot_general(moved, spread, (((0,), (0,)), ((), ())), preferred_element_type=f32)
    heads_shift[...] = shift[pl.ds(0, heads_shift.shape[0]), :]

    rows = 4 * SUB

    def scan_rows(i, carry, skip=0):
        h, p = carry
        at = pl.ds(pl.multiple_of(i * rows, rows), rows)
        decay, drive = gates(
            pre_r[at, :], pre_i[at, :], smoothed[at, :].astype(f32), b_decay[...], b_input[...], rate[...], shift[at, :]
        )
        known = lax.broadcasted_iota(jnp.int32, (SUB, width), 0) > 0
        for k in range(rows // SUB):
            a, b = decay[k * SUB : (k + 1) * SUB, :], drive[k * SUB : (k + 1) * SUB, :]
            if k < skip:
                a, b = jnp.where(known, a, 1.0), jnp.where(known, b, 0.0)
            h = a * h + b
            p = a * p
            here = pl.ds(pl.multiple_of(i * rows + k * SUB, SUB), SUB)
            h_out[here, :] = h
            p_out[here, :] = p
        return h, p

    start = (jnp.zeros((SUB, width), f32), jnp.ones((SUB, width), f32))
    h, p = lax.fori_loop(1, length // rows, scan_rows, scan_rows(0, start, taps - 1))
    ends_out[0] = p
    ends_out[1] = h


def head_kernel(
    inner, halo, conv, blocks, b_decay, b_input, rate, shift, ends,
    runs_out, heads_out, sent_out,
    near, smoothed, pre_r, pre_i,
):
    width = inner.shape[1]
    taps = conv.shape[0]
    near[pl.ds(0, HALO), :] = halo[...].astype(f32)
    near[pl.ds(HALO, HALO), :] = inner[pl.ds(0, 2 * HALO), :].astype(f32)[:HALO]
    smooth = near[pl.ds(HALO - taps + 1, HALO), :] * conv[0:1, :]
    for tap in range(1, taps):
        smooth = smooth + near[pl.ds(HALO - taps + 1 + tap, HALO), :] * conv[tap : tap + 1, :]
    smoothed[...] = jnp.concatenate([smooth, jnp.zeros_like(smooth)], axis=0).astype(bf16)

    def store(at, r, i):
        pre_r[:, at] = r[:HALO]
        pre_i[:, at] = i[:HALO]

    block_dots(smoothed, blocks, store)
    shifts = jnp.concatenate([shift[pl.ds(k * SUB, 1), :] for k in range(HALO)], axis=0)
    decay, drive = gates(
        pre_r[...], pre_i[...], smoothed[...].astype(f32)[:HALO], b_decay[...], b_input[...], rate[...], shifts
    )
    a_before, b_before = jnp.ones((1, width), f32), jnp.zeros((1, width), f32)
    for k in range(taps - 1):
        a_k = decay[k : k + 1, :]
        a_before, b_before = a_before * a_k, a_k * b_before + drive[k : k + 1, :]
        heads_out[0, k : k + 1, :] = a_before
        heads_out[1, k : k + 1, :] = b_before
    for s in range(SUB):
        runs_out[0, s : s + 1, :] = a_before
        runs_out[1, s : s + 1, :] = b_before
        a_s = ends[0, s : s + 1, :]
        a_before, b_before = a_before * a_s, a_s * b_before + ends[1, s : s + 1, :]
    pair = jnp.concatenate([a_before, b_before], axis=0)
    sent_out[...] = jnp.broadcast_to(pair[None], sent_out.shape)


def before_in(pieces, index):
    width = pieces.shape[2]
    a, b = jnp.ones((1, width), f32), jnp.zeros((1, width), f32)
    a_at, b_at = a, b
    for k in range(pieces.shape[0]):
        here = k == index
        a_at, b_at = jnp.where(here, a, a_at), jnp.where(here, b, b_at)
        a_k, b_k = pieces[k, 0:1, :], pieces[k, 1:2, :]
        a, b = a * a_k, a_k * b + b_k
    return (a_at, b_at), (a, b)


def plane_kernel(pieces, before_out, sent_out):
    index = lax.axis_index("sp_1") * lax.axis_size("sp_2") + lax.axis_index("sp_2")
    (a_at, b_at), (a, b) = before_in(pieces, index)
    before_out[...] = jnp.concatenate([a_at, b_at], axis=0)
    pair = jnp.concatenate([a, b], axis=0)
    sent_out[...] = jnp.broadcast_to(pair[None], sent_out.shape)


def back(gated, first):
    length = gated.shape[0]
    half, run = length // 2, length // SUB
    t = lax.broadcasted_iota(jnp.int32, (half, length), 0) + first
    c = lax.broadcasted_iota(jnp.int32, (half, length), 1)
    pick = jnp.where(t == (c & (SUB - 1)) * run + (c >> 3), 1.0, 0.0).astype(bf16)
    return dot(pick, gated[...]).astype(bf16)


def state_kernel(pieces, before, runs, heads, h, p, g, gated, theirs_out):
    (_, b_at), _ = before_in(pieces, lax.axis_index("sp_0"))
    carried = before[0:1, :] * b_at + before[1:2, :]
    start = runs[0] * carried + runs[1]
    length = h.shape[0]
    rows = 4 * SUB
    opening = heads[0] * carried + heads[1]
    first = [jnp.concatenate([opening[k : k + 1], start[1:]], axis=0) for k in range(heads.shape[1])]
    groups = rows // SUB

    def state_rows(i, starts):
        at = pl.ds(pl.multiple_of(i * rows, rows), rows)
        gated[at, :] = ((h[at, :] + p[at, :] * starts) * g[at, :]).astype(bf16)
        return starts

    state_rows(0, jnp.concatenate(first + [start] * (groups - len(first)), axis=0))
    starts = jnp.concatenate([start] * groups, axis=0)
    lax.fori_loop(1, length // rows, lambda i, _: (state_rows(i, starts), 0)[1], 0)
    theirs_out[...] = back(gated, (1 - lax.axis_index("tp")) * (length // 2))


def own_kernel(gated, w_mine, part):
    mine = back(gated, lax.axis_index("tp") * (gated.shape[0] // 2))
    part[...] = dot(mine, w_mine[...])


def out_kernel(part, theirs, w_theirs, out, block, sent):
    cols = block.shape[2]
    copies = []
    for i in range(block.shape[0]):
        at = pl.ds(i * cols, cols)
        block[i] = (part[:, at] + dot(theirs[...], w_theirs[:, at])).astype(bf16)
        copies.append(pltpu.make_async_copy(block.at[i], out.at[:, at], sent.at[i]))
        copies[i].start()
    for copy in copies:
        copy.wait()


VMEM = pl.BlockSpec(memory_space=pltpu.VMEM)


HBM = pl.BlockSpec(memory_space=pltpu.HBM)
ARGS = 11


def call(kernel, inputs, out_shape, scratch=(), out_specs=None):
    run = pl.pallas_call(
        kernel,
        out_shape=out_shape,
        out_specs=out_specs or jax.tree.map(lambda _: VMEM, out_shape),
        scratch_shapes=list(scratch),
        compiler_params=pltpu.CompilerParams(vmem_limit_bytes=32 * 1024 * 1024),
        in_specs=[VMEM] * inputs[0] + [HBM] * inputs[1],
    )

    def place(i, a):
        return pltpu.with_memory_space_constraint(a, pltpu.VMEM if i < inputs[0] else pltpu.HBM)

    return lambda *args: run(*(place(i, a) for i, a in enumerate(args)))


def step(
    tokens,
    norm_gain,
    in_weight,
    gate_weight,
    conv_weight,
    decay_gate_weight,
    decay_gate_bias,
    input_gate_weight,
    input_gate_bias,
    channel_decay_rate,
    forgetting_offset,
    out_weight,
):
    half, features = tokens.shape
    length = 2 * half
    width = in_weight.shape[1]
    heads, block = decay_gate_weight.shape[:2]
    count = lax.axis_size(SP)
    plane = lax.axis_size(PLANE)
    deep = lax.axis_size("sp_0")
    S = jax.ShapeDtypeStruct

    swap = [(0, 1), (1, 0)]
    other = lax.ppermute(tokens, "tp", swap)
    w_theirs = lax.ppermute(out_weight, "tp", swap)

    row = lambda v: v.reshape(1, -1)
    fetched = (
        row(norm_gain), in_weight, tokens, gate_weight,
        conv_weight, decay_gate_weight, row(decay_gate_bias),
        input_gate_weight, row(input_gate_bias), row(channel_decay_rate), forgetting_offset,
    )
    big = pltpu.VMEM
    like = lambda a: big(a.shape, a.dtype)
    square = big((length, width), f32)
    inner, tail, normed, *held = call(
        project_kernel,
        (1, ARGS),
        (
            big((length, width), bf16), big((HALO, width), bf16), big((length, features), bf16),
            *(like(a) for a in fetched[3:]),
        ),
        scratch=[
            *(like(a) for a in fetched[:3]),
            pltpu.SemaphoreType.DMA((ARGS,)),
            big((half, 128), f32),
            big((half, 128), f32),
        ],
    )(other, *fetched)
    w_gate, conv, w_decay, b_decay, w_input, b_input, rate, offset = held
    halo = lax.ppermute(tail, SP, [(s, s + 1) for s in range(count - 1)])
    taps = conv_weight.shape[0]
    h, p, g, ends, blocks, shift = call(
        scan_kernel,
        (10, 0),
        (
            square, square, square, big((2, SUB, width), f32),
            big((heads * block // 256, 256, 512), bf16), big((HALO * SUB, width), f32),
        ),
        scratch=[
            big((length, width), bf16), square, square, square,
            big((length + (taps - 1) * SUB, width), f32),
        ],
    )(inner, normed, w_gate, conv, w_decay, b_decay, w_input, b_input, rate, offset)
    runs, opening, sent = call(
        head_kernel,
        (9, 0),
        (big((2, SUB, width), f32), big((2, taps - 1, width), f32), big((plane, 2, width), f32)),
        scratch=[
            big((2 * HALO, width), f32), big((2 * HALO, width), bf16),
            big((HALO, width), f32), big((HALO, width), f32),
        ],
    )(inner, halo, conv, blocks, b_decay, b_input, rate, shift, ends)
    pieces = lax.all_to_all(sent, PLANE, split_axis=0, concat_axis=0, tiled=True)
    before, sent = call(plane_kernel, (1, 0), (big((2, width), f32), big((deep, 2, width), f32)))(pieces)
    pieces = lax.all_to_all(sent, "sp_0", split_axis=0, concat_axis=0, tiled=True)
    gated, theirs = call(
        state_kernel, (7, 0), (big((length, width), bf16), big((half, width), bf16))
    )(pieces, before, runs, opening, h, p, g)
    received = lax.ppermute(theirs, "tp", swap)
    part = call(own_kernel, (2, 0), big((half, features), f32))(gated, out_weight)
    cols = 512
    return call(
        out_kernel,
        (3, 0),
        S((half, features), bf16),
        scratch=(big((features // cols, half, cols), bf16), pltpu.SemaphoreType.DMA((features // cols,))),
        out_specs=HBM,
    )(part, received, w_theirs)


def solution(mesh):
    torus = Mesh(mesh.devices.reshape(8, 8, 4, mesh.shape["tp"]), SP_TP)
    placed = (
        P(SP_TP, None),
        P(),
        P(None, "tp"),
        P(None, "tp"),
        P(None, "tp"),
        P("tp", None, None),
        P("tp"),
        P("tp", None, None),
        P("tp"),
        P("tp"),
        P("tp", SP),
        P("tp", None),
    )
    return jax.shard_map(step, mesh=torus, in_specs=placed, out_specs=P(SP_TP, None), check_vma=False)
```

time: 66.6 us -> 64.7 us (0.971)
  starting transfers between devices: 19.9 us -> 17.3 us
  waiting for transfers between devices: 2.14 us -> 3.75 us
  local copies, waits for them, and re-layouts: 0.77 us -> 0.01 us
    ppermute x1, waiting for transfers between devices: 0.01 us -> 3.55 us  [step(): other = lax.ppermute(tokens, 'tp', swap)]
    ppermute x1, starting transfers between devices: 6.7 us -> 5.4 us  [step(): received = lax.ppermute(theirs, 'tp', swap)]
    ppermute x2 -> x1, starting transfers between devices: 2.57 us -> 1.29 us  [step(): halo = lax.ppermute(tail, SP, [(s, s + 1) for s in range(count - 1)])]
    ppermute x2 -> x1, waiting for transfers between devices: 1 us -> 0.01 us  [step(): halo = lax.ppermute(tail, SP, [(s, s + 1) for s in range(count - 1)])]
    ppermute x1, waiting for transfers between devices: 1.14 us -> 0.2 us  [step(): received = lax.ppermute(theirs, 'tp', swap)]
    slice x1 -> x0, local copies, waits for them, and re-layouts: 0.76 us -> none  [step(): tail = tokens[half - HALO:]]
    pallas_call x4 -> x7, Pallas kernels: 11 us -> 11.3 us  [call(): return lambda *args: run(*(place(i, a) for i, a in enumerate(args)))]
  transfers between devices with their start and end apart: 5 -> 4, of which waited for: 2 -> 2; matrix products, arithmetic and copies ran while one was open for 1% -> 0% of each run, Pallas kernels for 14% -> 15%
where the time goes in v1:
time: 64.7 us; the launch traced here: 64.4 us
  blocking collectives  31.9 us (49%)
  starting transfers between devices  17.3 us (27%)
  Pallas kernels  11.3 us (17%)
  waiting for transfers between devices  3.75 us (6%)
    all_to_all x1, blocking collectives, step(): lax.all_to_all(sent, 'sp_0', split_axis=0, concat_axis=0, tiled=True)  16.7 us
    all_to_all x1, blocking collectives, step(): lax.all_to_all(sent, PLANE, split_axis=0, concat_axis=0, tiled=True)  15.1 us
    pallas_call x7, Pallas kernels, call(): return lambda *args: run(*(place(i, a) for i, a in enumerate(args)))  11.3 us
    ppermute x1, starting transfers between devices, step(): w_theirs = lax.ppermute(out_weight, 'tp', swap)  8.74 us
    ppermute x1, starting transfers between devices, step(): received = lax.ppermute(theirs, 'tp', swap)  5.4 us
    ppermute x1, waiting for transfers between devices, step(): other = lax.ppermute(tokens, 'tp', swap)  3.55 us
    ppermute x1, starting transfers between devices, step(): other = lax.ppermute(tokens, 'tp', swap)  1.92 us
  transfers between devices with their start and end apart: 4, of which 2 were waited for; matrix products, arithmetic and copies ran while one was open for 0% of the time, Pallas kernels for 15%

profile of v1, /device:TPU:1, one launch (start us, length us, event | category | flops | bytes accessed | tf_op | source)
XLA Modules:
  0.0 64.4 jit_solution(3459186515732859860)
XLA Ops:
  0.0 8.7 %collective-permute-start.3 = (bf16[512,2048]{1,0:T(8,128)(2,1)}, bf16[512,2048]{1,0:T(8,128)(2,1)S(1)}, u32[]{:S(2)}, u32[]{:S(2)}) collective-permute-start(bf16[512,2048]{1,0:T(8,128)(2,1)} %w_mine.1), channel_id=1, source_target_pairs={{0,1},{1,0},{2,3},{3,2},{4,5},{5,4},{6,7},{7,6},{8,9},{9,8},{10,11... | collective-permute-start | bytes 6291464 | tf_op jit(solution)/shard_map/ppermute | solution.py:338
  8.7 1.9 %collective-permute-start = (bf16[256,2048]{1,0:T(8,128)(2,1)}, bf16[256,2048]{1,0:T(8,128)(2,1)S(1)}, u32[]{:S(2)}, u32[]{:S(2)}) collective-permute-start(bf16[256,2048]{1,0:T(8,128)(2,1)} %refs_2_.1), channel_id=1, source_target_pairs={{0,1},{1,0},{2,3},{3,2},{4,5},{5,4},{6,7},{7,6},{8,9},{9,8},{10,11... | collective-permute-start | bytes 3145736 | tf_op jit(solution)/shard_map/ppermute | solution.py:337
  10.7 3.5 %collective-permute-done.other = bf16[256,2048]{1,0:T(8,128)(2,1)S(1)} collective-permute-done((bf16[256,2048]{1,0:T(8,128)(2,1)}, bf16[256,2048]{1,0:T(8,128)(2,1)S(1)}, u32[]{:S(2)}, u32[]{:S(2)}) %collective-permute-start) | collective-permute-done | bytes 1048608 | tf_op jit(solution)/shard_map/ppermute | solution.py:337
  14.2 3.7 %shard_map.118 = (bf16[512,512]{1,0:T(8,128)(2,1)S(1)}, bf16[8,512]{1,0:T(8,128)(2,1)S(1)}, bf16[512,2048]{1,0:T(8,128)(2,1)S(1)}, bf16[2048,512]{1,0:T(8,128)(2...) custom-call(bf16[256,2048]{1,0:T(8,128)(2,1)S(1)} %collective-permut, ...), custom_call_target="tpu_custom_call" | custom-call | tf_op jit(solution)/shard_map/pallas_call | solution.py:310
  18.0 1.3 %collective-permute-start.1 = (bf16[8,512]{1,0:T(8,128)(2,1)S(1)}, bf16[8,512]{1,0:T(8,128)(2,1)S(1)}, u32[]{:S(2)}, u32[]{:S(2)}) collective-permute-start(bf16[8,512]{1,0:T(8,128)(2,1)S(1)} %get-tuple-element.30), channel_id=1, source_target_pairs={{0,2},{2,4},{4,6},{6,8},{8,10},{10,12},{12,14},{14,16},{16,18},{18... | collective-permute-start | bytes 24584 | tf_op jit(solution)/shard_map/ppermute | solution.py:364
  19.3 4.3 %shard_map.119 = (f32[512,512]{1,0:T(8,128)S(1)}, f32[512,512]{1,0:T(8,128)S(1)}, f32[512,512]{1,0:T(8,128)S(1)}, f32[2,8,512]{2,1,0:T(8,128)S(1)}, bf16[2,256,5...) custom-call(bf16[512,512]{1,0:T(8,128)(2,1)S(1)} %get-tuple-element.29.inner, ...), custom_call_target="tpu_custom_call" | custom-call | tf_op jit(solution)/shard_map/pallas_call | solution.py:310
  23.6 0.0 collective-permute-done.1.halo
  23.6 0.3 shard_map.120
  23.9 0.0 copy-start
  23.9 15.1 %all_to_all.10.pieces = f32[32,2,512]{2,1,0:T(2,128)S(1)} all-to-all(f32[32,2,512]{2,1,0:T(2,128)S(1)} %get-tuple-element.43), channel_id=1, replica_groups=mesh['sp_0'=8,'sp_1'=8,'sp_2'=4,'tp'=2] {'sp_1','sp_2'}, dimensions={0} | all-to-all | bytes 262144 | tf_op jit(solution)/shard_map/all_to_all | solution.py:387
  39.0 0.1 shard_map.121
  39.1 16.7 %all_to_all.11.pieces = f32[8,2,512]{2,1,0:T(2,128)S(1)} all-to-all(f32[8,2,512]{2,1,0:T(2,128)S(1)} %get-tuple-element.44), channel_id=1, replica_groups=mesh['sp_0'=8,'sp_1'=8,'sp_2'=4,'tp'=2] {'sp_0'}, dimensions={0} | all-to-all | bytes 65536 | tf_op jit(solution)/shard_map/all_to_all | solution.py:389
  55.8 0.6 shard_map.122
  56.4 5.4 %collective-permute-start.2 = (bf16[256,512]{1,0:T(8,128)(2,1)S(1)}, bf16[256,512]{1,0:T(8,128)(2,1)S(1)}, u32[]{:S(2)}, u32[]{:S(2)}) collective-permute-start(bf16[256,512]{1,0:T(8,128)(2,1)S(1)} %get-tuple-element.52), channel_id=1, source_target_pairs={{0,1},{1,0},{2,3},{3,2},{4,5},{5,4},{6,7},{7,6},{8,9},{9,8},{10,11... | collective-permute-start | bytes 786440 | tf_op jit(solution)/shard_map/ppermute | solution.py:393
  61.8 0.0 copy-done
  61.8 0.9 %shard_map.123.part = f32[256,2048]{1,0:T(8,128)S(1)} custom-call(bf16[512,512]{1,0:T(8,128)(2,1)S(1)} %get-tuple-element.51.gated, bf16[512,2048]{1,0:T(8,128)(2,1)S(1)} %copy-done), custom_call_target="tpu_custom_call" | custom-call | tf_op jit(solution)/shard_map/pallas_call | solution.py:310
  62.7 0.2 collective-permute-done.2.theirs
  62.9 0.0 collective-permute-done.3.w_theirs
  62.9 1.5 %shard_map.124 = bf16[256,2048]{1,0:T(8,128)(2,1)} custom-call(f32[256,2048]{1,0:T(8,128)S(1)} %shard_map.123.part, bf16[256,512]{1,0:T(8,128)(2,1)S(1)} %collective-permute-done.2.theirs, bf16[512,2048]{1,0:T(8,128)(2,1)S(1)} %collective-permute-done.3.w_theirs), custom_call_target="tpu_custom_call" | custom-call | tf_op jit(solution)/shard_map/pallas_call | solution.py:310
Async XLA Ops:
  0.0 62.9 %collective-permute-start.3 = (bf16[512,2048]{1,0:T(8,128)(2,1)}, bf16[512,2048]{1,0:T(8,128)(2,1)S(1)}, u32[]{:S(2)}, u32[]{:S(2)}) collective-permute-start(bf16[512,2048]{1,0:T(8,128)(2,1)} %w_mine.1), channel_id=1, source_target_pairs={{0,1},{1,0},{2,3},{3,2},{4,5},{5,4},{6,7},{7,6},{8,9},{9,8},{10,11... | collective-permute-start | bytes 6291464 | tf_op jit(solution)/shard_map/ppermute | solution.py:338
  8.7 5.5 %collective-permute-start = (bf16[256,2048]{1,0:T(8,128)(2,1)}, bf16[256,2048]{1,0:T(8,128)(2,1)S(1)}, u32[]{:S(2)}, u32[]{:S(2)}) collective-permute-start(bf16[256,2048]{1,0:T(8,128)(2,1)} %refs_2_.1), channel_id=1, source_target_pairs={{0,1},{1,0},{2,3},{3,2},{4,5},{5,4},{6,7},{7,6},{8,9},{9,8},{10,11... | collective-permute-start | bytes 3145736 | tf_op jit(solution)/shard_map/ppermute | solution.py:337
  18.0 5.6 %collective-permute-start.1 = (bf16[8,512]{1,0:T(8,128)(2,1)S(1)}, bf16[8,512]{1,0:T(8,128)(2,1)S(1)}, u32[]{:S(2)}, u32[]{:S(2)}) collective-permute-start(bf16[8,512]{1,0:T(8,128)(2,1)S(1)} %get-tuple-element.30), channel_id=1, source_target_pairs={{0,2},{2,4},{4,6},{6,8},{8,10},{10,12},{12,14},{14,16},{16,18},{18... | collective-permute-start | bytes 24584 | tf_op jit(solution)/shard_map/ppermute | solution.py:364
  23.9 37.9 %copy-start = (bf16[512,2048]{1,0:T(8,128)(2,1)S(1)}, bf16[512,2048]{1,0:T(8,128)(2,1)}, u32[]{:S(2)}) copy-start(bf16[512,2048]{1,0:T(8,128)(2,1)} %w_mine.1) | copy-start | bytes 6291460
  56.4 6.5 %collective-permute-start.2 = (bf16[256,512]{1,0:T(8,128)(2,1)S(1)}, bf16[256,512]{1,0:T(8,128)(2,1)S(1)}, u32[]{:S(2)}, u32[]{:S(2)}) collective-permute-start(bf16[256,512]{1,0:T(8,128)(2,1)S(1)} %get-tuple-element.52), channel_id=1, source_target_pairs={{0,1},{1,0},{2,3},{3,2},{4,5},{5,4},{6,7},{7,6},{8,9},{9,8},{10,11... | collective-permute-start | bytes 786440 | tf_op jit(solution)/shard_map/ppermute | solution.py:393

commit v2 on v1

--- a/solution.py
+++ b/solution.py
@@ -24,22 +24,16 @@
     return 1.0 / (1.0 + jnp.exp(-x))
 
 
-def project_kernel(other, *refs):
-    stored, refs = refs[:ARGS], refs[ARGS:]
-    inner, tail, normed, *held = refs[: ARGS]
-    gain, w_in, own, arrived, middle, scale = refs[ARGS:]
-    held = (gain, w_in, own, *held)
-    copies = [pltpu.make_async_copy(a, b, arrived.at[i]) for i, (a, b) in enumerate(zip(stored, held))]
-    half, features = own.shape
-    tp = lax.axis_index("tp")
+def norm_tokens(source, target, gain, middle, scale, ready=None):
+    half, features = source.shape
     step, lanes = 32, 128
 
-    def tiles(source, r):
+    def tiles(r):
         return [source[r, t : t + lanes].astype(f32) for t in range(0, features, lanes)]
 
     def by_rows(one):
         def rows(i, _):
-            one(pl.multiple_of(i * step, step))
+            one(pl.ds(pl.multiple_of(i * step, step), step))
             return 0
 
         lax.fori_loop(0, half // step, rows, 0)
@@ -47,44 +41,54 @@
     def over_features(stat):
         return jnp.broadcast_to(jnp.sum(stat[...], axis=1, keepdims=True) * (1.0 / features), stat.shape)
 
-    def norm_tokens(source, base, ready=None):
-        def add_up(i):
-            r = pl.ds(i, step)
-            middle[r, :] = sum(tiles(source, r))
-
-        by_rows(add_up)
-        middle[...] = over_features(middle)
-
-        def add_squares(i):
-            r = pl.ds(i, step)
-            m = middle[r, :]
-            scale[r, :] = sum((x - m) * (x - m) for x in tiles(source, r))
-
-        by_rows(add_squares)
-        scale[...] = lax.rsqrt(over_features(scale) + EPSILON)
-        if ready is not None:
-            ready.wait()
-
-        def write(i):
-            r = pl.ds(i, step)
-            m, k = middle[r, :], scale[r, :]
-            d = pl.ds(pl.multiple_of(base + i, step), step)
-            for t, x in zip(range(0, features, lanes), tiles(source, r)):
-                normed[d, t : t + lanes] = ((x - m) * k * gain[:, t : t + lanes]).astype(bf16)
-
-        by_rows(write)
-
-    for i in (0, 2, 1, *range(3, ARGS)):
+    def add_up(r):
+        middle[r, :] = sum(tiles(r))
+
+    by_rows(add_up)
+    middle[...] = over_features(middle)
+
+    def add_squares(r):
+        m = middle[r, :]
+        scale[r, :] = sum((x - m) * (x - m) for x in tiles(r))
+
+    by_rows(add_squares)
+    scale[...] = lax.rsqrt(over_features(scale) + EPSILON)
+    if ready is not None:
+        ready.wait()
+
+    def write(r):
+        m, k = middle[r, :], scale[r, :]
+        for t, x in zip(range(0, features, lanes), tiles(r)):
+            target[r, t : t + lanes] = ((x - m) * k * gain[:, t : t + lanes]).astype(bf16)
+
+    by_rows(write)
+
+
+def own_tokens_kernel(*refs):
+    stored, refs = refs[:ARGS], refs[ARGS:]
+    inner, normed, *held = refs[: ARGS + 1]
+    own, arrived, middle, scale = refs[ARGS + 1 :]
+    held.insert(2, own)
+    gain, w_in = held[:2]
+    copies = [pltpu.make_async_copy(a, b, arrived.at[i]) for i, (a, b) in enumerate(zip(stored, held))]
+    for i in (2, 0, 1, *range(3, ARGS)):
         copies[i].start()
-    norm_tokens(other, (1 - tp) * half, copies[0])
     copies[2].wait()
-    norm_tokens(own, tp * half)
+    norm_tokens(own, normed, gain, middle, scale, copies[0])
     copies[1].wait()
-    both = dot(normed[...], w_in[...]).astype(bf16)
-    inner[...] = both
-    tail[...] = both[2 * half - HALO :]
+    inner[...] = dot(normed[...], w_in[...]).astype(bf16)
     for copy in copies[3:]:
         copy.wait()
+
+
+def other_tokens_kernel(other, gain, w_in, inner_own, inner, tail, normed, middle, scale):
+    half = other.shape[0]
+    tp = lax.axis_index("tp")
+    norm_tokens(other, normed, gain, middle, scale)
+    inner[pl.ds(pl.multiple_of(tp * half, half), half), :] = inner_own[...]
+    there = pl.ds(pl.multiple_of((1 - tp) * half, half), half)
+    inner[there, :] = dot(normed[...], w_in[...]).astype(bf16)
+    tail[...] = inner[pl.ds(2 * half - 2 * HALO, 2 * HALO), :].astype(f32)[HALO:].astype(bf16)
 
 
 def gates(pre_r, pre_i, x, b_decay, b_input, rate, shift):
@@ -105,9 +109,9 @@
 
 
 def scan_kernel(
-    inner, normed, w_gate, conv, w_decay, b_decay, w_input, b_input, rate, offset,
+    inner, normed_own, normed_other, w_gate, conv, w_decay, b_decay, w_input, b_input, rate, offset,
     h_out, p_out, g_out, ends_out, blocks, heads_shift,
-    smoothed, pre_r, pre_i, shift, extended,
+    smoothed, pre_r, pre_i, shift, extended, gate,
 ):
     length, width = inner.shape
     run = length // SUB
@@ -122,8 +126,6 @@
     order = picks(length, 0)
     extended[pl.ds(lead, length), :] = dot(order, inner[...])
     extended[pl.ds(0, lead), :] = dot(picks(lead, 1 - taps), inner[...])
-    gate = dot(normed[...], w_gate[...]).astype(bf16)
-    g_out[...] = jax.nn.gelu(dot(order, gate))
 
     smooth = extended[pl.ds(0, length), :] * conv[0:1, :]
     for tap in range(1, taps):
@@ -177,7 +179,15 @@
         return h, p
 
     start = (jnp.zeros((SUB, width), f32), jnp.ones((SUB, width), f32))
-    h, p = lax.fori_loop(1, length // rows, scan_rows, scan_rows(0, start, taps - 1))
+    h, p = start
+    half, blocks_half = length // 2, length // rows // 2
+    tp = lax.axis_index("tp")
+    for c, (normed, place) in enumerate(((normed_own, tp), (normed_other, 1 - tp))):
+        at = pl.ds(pl.multiple_of(place * half, half), half)
+        gate[at, :] = dot(normed[...], w_gate[...]).astype(bf16)
+        for i in range(c * blocks_half, (c + 1) * blocks_half):
+            h, p = scan_rows(i, (h, p), 0 if i else taps - 1)
+    g_out[...] = jax.nn.gelu(dot(order, gate[...]))
     ends_out[0] = p
     ends_out[1] = h
 
@@ -249,7 +259,7 @@
     return dot(pick, gated[...]).astype(bf16)
 
 
-def state_kernel(pieces, before, runs, heads, h, p, g, gated, theirs_out):
+def state_kernel(pieces, before, runs, heads, h, p, g, w_mine, gated, theirs_out):
     (_, b_at), _ = before_in(pieces, lax.axis_index("sp_0"))
     carried = before[0:1, :] * b_at + before[1:2, :]
     start = runs[0] * carried + runs[1]
@@ -267,7 +277,8 @@
     state_rows(0, jnp.concatenate(first + [start] * (groups - len(first)), axis=0))
     starts = jnp.concatenate([start] * groups, axis=0)
     lax.fori_loop(1, length // rows, lambda i, _: (state_rows(i, starts), 0)[1], 0)
-    theirs_out[...] = back(gated, (1 - lax.axis_index("tp")) * (length // 2))
+    theirs = back(gated, (1 - lax.axis_index("tp")) * (length // 2))
+    theirs_out[...] = dot(theirs, w_mine[...]).astype(bf16)
 
 
 def own_kernel(gated, w_mine, part):
@@ -275,13 +286,13 @@
     part[...] = dot(mine, w_mine[...])
 
 
-def out_kernel(part, theirs, w_theirs, out, block, sent):
-    cols = block.shape[2]
+def out_kernel(part, received, out, block, sent):
+    rows = block.shape[1]
     copies = []
     for i in range(block.shape[0]):
-        at = pl.ds(i * cols, cols)
-        block[i] = (part[:, at] + dot(theirs[...], w_theirs[:, at])).astype(bf16)
-        copies.append(pltpu.make_async_copy(block.at[i], out.at[:, at], sent.at[i]))
+        at = pl.ds(i * rows, rows)
+        block[i] = (part[at, :] + received[at, :].astype(f32)).astype(bf16)
+        copies.append(pltpu.make_async_copy(block.at[i], out.at[at, :], sent.at[i]))
         copies[i].start()
     for copy in copies:
         copy.wait()
@@ -335,7 +346,6 @@
 
     swap = [(0, 1), (1, 0)]
     other = lax.ppermute(tokens, "tp", swap)
-    w_theirs = lax.ppermute(out_weight, "tp", swap)
 
     row = lambda v: v.reshape(1, -1)
     fetched = (
@@ -346,35 +356,37 @@
     big = pltpu.VMEM
     like = lambda a: big(a.shape, a.dtype)
     square = big((length, width), f32)
-    inner, tail, normed, *held = call(
-        project_kernel,
-        (1, ARGS),
+    stats = [big((half, 128), f32), big((half, 128), f32)]
+    inner_own, normed_own, gain, w_in, *held = call(
+        own_tokens_kernel,
+        (0, ARGS),
         (
-            big((length, width), bf16), big((HALO, width), bf16), big((length, features), bf16),
-            *(like(a) for a in fetched[3:]),
+            big((half, width), bf16), big((half, features), bf16),
+            *(like(a) for i, a in enumerate(fetched) if i != 2),
         ),
-        scratch=[
-            *(like(a) for a in fetched[:3]),
-            pltpu.SemaphoreType.DMA((ARGS,)),
-            big((half, 128), f32),
-            big((half, 128), f32),
-        ],
-    )(other, *fetched)
+        scratch=[like(tokens), pltpu.SemaphoreType.DMA((ARGS,)), *stats],
+    )(*fetched)
+    inner, tail, normed_other = call(
+        other_tokens_kernel,
+        (4, 0),
+        (big((length, width), bf16), big((HALO, width), bf16), big((half, features), bf16)),
+        scratch=stats,
+    )(other, gain, w_in, inner_own)
     w_gate, conv, w_decay, b_decay, w_input, b_input, rate, offset = held
     halo = lax.ppermute(tail, SP, [(s, s + 1) for s in range(count - 1)])
     taps = conv_weight.shape[0]
     h, p, g, ends, blocks, shift = call(
         scan_kernel,
-        (10, 0),
+        (11, 0),
         (
             square, square, square, big((2, SUB, width), f32),
             big((heads * block // 256, 256, 512), bf16), big((HALO * SUB, width), f32),
         ),
         scratch=[
             big((length, width), bf16), square, square, square,
-            big((length + (taps - 1) * SUB, width), f32),
+            big((length + (taps - 1) * SUB, width), f32), big((length, width), bf16),
         ],
-    )(inner, normed, w_gate, conv, w_decay, b_decay, w_input, b_input, rate, offset)
+    )(inner, normed_own, normed_other, w_gate, conv, w_decay, b_decay, w_input, b_input, rate, offset)
     runs, opening, sent = call(
         head_kernel,
         (9, 0),
@@ -388,18 +400,18 @@
     before, sent = call(plane_kernel, (1, 0), (big((2, width), f32), big((deep, 2, width), f32)))(pieces)
     pieces = lax.all_to_all(sent, "sp_0", split_axis=0, concat_axis=0, tiled=True)
     gated, theirs = call(
-        state_kernel, (7, 0), (big((length, width), bf16), big((half, width), bf16))
-    )(pieces, before, runs, opening, h, p, g)
+        state_kernel, (8, 0), (big((length, width), bf16), big((half, features), bf16))
+    )(pieces, before, runs, opening, h, p, g, out_weight)
     received = lax.ppermute(theirs, "tp", swap)
     part = call(own_kernel, (2, 0), big((half, features), f32))(gated, out_weight)
-    cols = 512
+    rows = 64
     return call(
         out_kernel,
-        (3, 0),
+        (2, 0),
         S((half, features), bf16),
-        scratch=(big((features // cols, half, cols), bf16), pltpu.SemaphoreType.DMA((features // cols,))),
+        scratch=(big((half // rows, rows, features), bf16), pltpu.SemaphoreType.DMA((half // rows,))),
         out_specs=HBM,
-    )(part, received, w_theirs)
+    )(part, received)
 
 
 def solution(mesh):

time: 64.7 us -> 61.3 us (0.947)
  waiting for transfers between devices: 3.75 us -> 1.34 us
  starting transfers between devices: 17.3 us -> 15.3 us
  Pallas kernels: 11.3 us -> 12.5 us
    ppermute x1 -> x0, starting transfers between devices: 8.74 us -> none  [step(): w_theirs = lax.ppermute(out_weight, 'tp', swap)]
    ppermute x1, starting transfers between devices: 1.92 us -> 8.73 us  [step(): other = lax.ppermute(tokens, 'tp', swap)]
    ppermute x1, waiting for transfers between devices: 3.55 us -> 0.01 us  [step(): other = lax.ppermute(tokens, 'tp', swap)]
    pallas_call x7 -> x8, Pallas kernels: 11.3 us -> 12.5 us  [call(): return lambda *args: run(*(place(i, a) for i, a in enumerate(args)))]
    ppermute x1, waiting for transfers between devices: 0.2 us -> 1.34 us  [step(): received = lax.ppermute(theirs, 'tp', swap)]
  transfers between devices with their start and end apart: 4 -> 3, of which waited for: 2 -> 1; matrix products, arithmetic and copies ran while one was open for 0% -> 0% of each run, Pallas kernels for 15% -> 13%
where the time goes in v2:
time: 61.3 us; the launch traced here: 61.1 us
  blocking collectives  31.8 us (52%)
  starting transfers between devices  15.3 us (25%)
  Pallas kernels  12.5 us (20%)
  waiting for transfers between devices  1.34 us (2%)
    all_to_all x1, blocking collectives, step(): lax.all_to_all(sent, 'sp_0', split_axis=0, concat_axis=0, tiled=True)  16.7 us
    all_to_all x1, blocking collectives, step(): lax.all_to_all(sent, PLANE, split_axis=0, concat_axis=0, tiled=True)  15.1 us
    pallas_call x8, Pallas kernels, call(): return lambda *args: run(*(place(i, a) for i, a in enumerate(args)))  12.5 us
    ppermute x1, starting transfers between devices, step(): other = lax.ppermute(tokens, 'tp', swap)  8.73 us
    ppermute x1, starting transfers between devices, step(): received = lax.ppermute(theirs, 'tp', swap)  5.26 us
    ppermute x1, waiting for transfers between devices, step(): received = lax.ppermute(theirs, 'tp', swap)  1.34 us
    ppermute x1, starting transfers between devices, step(): halo = lax.ppermute(tail, SP, [(s, s + 1) for s in range(count - 1)])  1.29 us
  transfers between devices with their start and end apart: 3, of which 1 were waited for; matrix products, arithmetic and copies ran while one was open for 0% of the time, Pallas kernels for 13%

profile of v2, /device:TPU:1, one launch (start us, length us, event | category | flops | bytes accessed | tf_op | source)
XLA Modules:
  0.0 61.1 jit_solution(14592400374634755220)
XLA Ops:
  0.0 8.7 %collective-permute-start = (bf16[256,2048]{1,0:T(8,128)(2,1)}, bf16[256,2048]{1,0:T(8,128)(2,1)S(1)}, u32[]{:S(2)}, u32[]{:S(2)}) collective-permute-start(bf16[256,2048]{1,0:T(8,128)(2,1)} %refs_2_.1), channel_id=1, source_target_pairs={{0,1},{1,0},{2,3},{3,2},{4,5},{5,4},{6,7},{7,6},{8,9},{9,8},{10,11... | collective-permute-start | bytes 3145736 | tf_op jit(solution)/shard_map/ppermute | solution.py:348
  8.7 3.2 %shard_map.118 = (bf16[256,512]{1,0:T(8,128)(2,1)S(1)}, bf16[256,2048]{1,0:T(8,128)(2,1)S(1)}, f32[1,2048]{1,0:T(1,128)S(1)}, bf16[2048,512]{1,0:T(8,128)(2,1)S(...) custom-call(f32[1,2048]{1,0:T(1,128)} %bitcast.4, ...), custom_call_target="tpu_custom_call" | custom-call | tf_op jit(solution)/shard_map/pallas_call | solution.py:321
  11.9 0.0 collective-permute-done.other
  11.9 1.9 %shard_map.119 = (bf16[512,512]{1,0:T(8,128)(2,1)S(1)}, bf16[8,512]{1,0:T(8,128)(2,1)S(1)}, bf16[256,2048]{1,0:T(8,128)(2,1)S(1)}) custom-call(bf16[256,2048]{1,0:T(8,128)(2,1)S(1)} %collective-permute-done.other, f32[1,2048]{1,0:T(1,128)S(1)} %get-tuple-element.33.gain, bf16[2048,512]{1,0:T(8,128)(2,1)S(1)} %get-tuple-element.34.w_in, ...), custom_call_target="tpu_custom_call" | custom-call | tf_op jit(solution)/shard_map/pallas_call | solution.py:321
  13.8 1.3 %collective-permute-start.1 = (bf16[8,512]{1,0:T(8,128)(2,1)S(1)}, bf16[8,512]{1,0:T(8,128)(2,1)S(1)}, u32[]{:S(2)}, u32[]{:S(2)}) collective-permute-start(bf16[8,512]{1,0:T(8,128)(2,1)S(1)} %get-tuple-element.37), channel_id=1, source_target_pairs={{0,2},{2,4},{4,6},{6,8},{8,10},{10,12},{12,14},{14,16},{16,18},{18... | collective-permute-start | bytes 24584 | tf_op jit(solution)/shard_map/ppermute | solution.py:376
  15.1 0.0 copy-start
  15.1 3.9 %shard_map.120 = (f32[512,512]{1,0:T(8,128)S(1)}, f32[512,512]{1,0:T(8,128)S(1)}, f32[512,512]{1,0:T(8,128)S(1)}, f32[2,8,512]{2,1,0:T(8,128)S(1)}, bf16[2,256,5...) custom-call(bf16[512,512]{1,0:T(8,128)(2,1)S(1)} %get-tuple-element.36.inner, ...), custom_call_target="tpu_custom_call" | custom-call | tf_op jit(solution)/shard_map/pallas_call | solution.py:321
  19.0 0.0 collective-permute-done.1.halo
  19.0 0.3 shard_map.121
  19.3 15.1 %all_to_all.10.pieces = f32[32,2,512]{2,1,0:T(2,128)S(1)} all-to-all(f32[32,2,512]{2,1,0:T(2,128)S(1)} %get-tuple-element.51), channel_id=1, replica_groups=mesh['sp_0'=8,'sp_1'=8,'sp_2'=4,'tp'=2] {'sp_1','sp_2'}, dimensions={0} | all-to-all | bytes 262144 | tf_op jit(solution)/shard_map/all_to_all | solution.py:399
  34.4 0.1 shard_map.122
  34.5 16.7 %all_to_all.11.pieces = f32[8,2,512]{2,1,0:T(2,128)S(1)} all-to-all(f32[8,2,512]{2,1,0:T(2,128)S(1)} %get-tuple-element.52), channel_id=1, replica_groups=mesh['sp_0'=8,'sp_1'=8,'sp_2'=4,'tp'=2] {'sp_0'}, dimensions={0} | all-to-all | bytes 65536 | tf_op jit(solution)/shard_map/all_to_all | solution.py:401
  51.2 0.0 copy-done
  51.2 1.3 %shard_map.123 = (bf16[512,512]{1,0:T(8,128)(2,1)S(1)}, bf16[256,2048]{1,0:T(8,128)(2,1)S(1)}) custom-call(f32[8,2,512]{2,1,0:T(2,128)S(1)} %all_to_all.11.pieces, f32[2,512]{1,0:T(2,128)S(1)} %get-tuple-element.53.before, f32[2,8,512]{2,1,0:T(8,128)S(1)} %get-tuple-element.54.runs, f32[2,3,512]{2,1,0:T(4,128)S(1)} %get-tuple-element.55.heads, ...), custom_call_target="tpu_custom_call" | custom-call | tf_op jit(solution)/shard_map/pallas_call | solution.py:321
  52.5 5.3 %collective-permute-start.2 = (bf16[256,2048]{1,0:T(8,128)(2,1)S(1)}, bf16[256,2048]{1,0:T(8,128)(2,1)S(1)}, u32[]{:S(2)}, u32[]{:S(2)}) collective-permute-start(bf16[256,2048]{1,0:T(8,128)(2,1)S(1)} %get-tuple-element.60), channel_id=1, source_target_pairs={{0,1},{1,0},{2,3},{3,2},{4,5},{5,4},{6,7},{7,6},{8,9},{9,8},{10,11... | collective-permute-start | bytes 3145736 | tf_op jit(solution)/shard_map/ppermute | solution.py:405
  57.8 0.9 %shard_map.124.part = f32[256,2048]{1,0:T(8,128)S(1)} custom-call(bf16[512,512]{1,0:T(8,128)(2,1)S(1)} %get-tuple-element.59.gated, bf16[512,2048]{1,0:T(8,128)(2,1)S(1)} %copy-done), custom_call_target="tpu_custom_call" | custom-call | tf_op jit(solution)/shard_map/pallas_call | solution.py:321
  58.7 1.3 %collective-permute-done.2.received = bf16[256,2048]{1,0:T(8,128)(2,1)S(1)} collective-permute-done((bf16[256,2048]{1,0:T(8,128)(2,1)S(1)}, bf16[256,2048]{1,0:T(8,128)(2,1)S(1)}, u32[]{:S(2)}, u32[]{:S(2)}) %collective-permute-start.2) | collective-permute-done | bytes 1048608 | tf_op jit(solution)/shard_map/ppermute | solution.py:405
  60.0 1.0 %shard_map.125 = bf16[256,2048]{1,0:T(8,128)(2,1)} custom-call(f32[256,2048]{1,0:T(8,128)S(1)} %shard_map.124.part, bf16[256,2048]{1,0:T(8,128)(2,1)S(1)} %collective-permute-done.2.received), custom_call_target="tpu_custom_call" | custom-call | tf_op jit(solution)/shard_map/pallas_call | solution.py:321
Async XLA Ops:
  0.0 11.9 %collective-permute-start = (bf16[256,2048]{1,0:T(8,128)(2,1)}, bf16[256,2048]{1,0:T(8,128)(2,1)S(1)}, u32[]{:S(2)}, u32[]{:S(2)}) collective-permute-start(bf16[256,2048]{1,0:T(8,128)(2,1)} %refs_2_.1), channel_id=1, source_target_pairs={{0,1},{1,0},{2,3},{3,2},{4,5},{5,4},{6,7},{7,6},{8,9},{9,8},{10,11... | collective-permute-start | bytes 3145736 | tf_op jit(solution)/shard_map/ppermute | solution.py:348
  13.8 5.2 %collective-permute-start.1 = (bf16[8,512]{1,0:T(8,128)(2,1)S(1)}, bf16[8,512]{1,0:T(8,128)(2,1)S(1)}, u32[]{:S(2)}, u32[]{:S(2)}) collective-permute-start(bf16[8,512]{1,0:T(8,128)(2,1)S(1)} %get-tuple-element.37), channel_id=1, source_target_pairs={{0,2},{2,4},{4,6},{6,8},{8,10},{10,12},{12,14},{14,16},{16,18},{18... | collective-permute-start | bytes 24584 | tf_op jit(solution)/shard_map/ppermute | solution.py:376
  15.1 36.1 %copy-start = (bf16[512,2048]{1,0:T(8,128)(2,1)S(1)}, bf16[512,2048]{1,0:T(8,128)(2,1)}, u32[]{:S(2)}) copy-start(bf16[512,2048]{1,0:T(8,128)(2,1)} %w_mine.3) | copy-start | bytes 6291460
  52.5 7.5 %collective-permute-start.2 = (bf16[256,2048]{1,0:T(8,128)(2,1)S(1)}, bf16[256,2048]{1,0:T(8,128)(2,1)S(1)}, u32[]{:S(2)}, u32[]{:S(2)}) collective-permute-start(bf16[256,2048]{1,0:T(8,128)(2,1)S(1)} %get-tuple-element.60), channel_id=1, source_target_pairs={{0,1},{1,0},{2,3},{3,2},{4,5},{5,4},{6,7},{7,6},{8,9},{9,8},{10,11... | collective-permute-start | bytes 3145736 | tf_op jit(solution)/shard_map/ppermute | solution.py:405

commit v3 on v2

--- a/solution.py
+++ b/solution.py
@@ -20,10 +20,6 @@
     return jnp.dot(a, b, preferred_element_type=f32)
 
 
-def sigmoid(x):
-    return 1.0 / (1.0 + jnp.exp(-x))
-
-
 def norm_tokens(source, target, gain, middle, scale, ready=None):
     half, features = source.shape
     step, lanes = 32, 128
@@ -64,24 +60,26 @@
     by_rows(write)
 
 
-def own_tokens_kernel(*refs):
-    stored, refs = refs[:ARGS], refs[ARGS:]
-    inner, normed, *held = refs[: ARGS + 1]
-    own, arrived, middle, scale = refs[ARGS + 1 :]
-    held.insert(2, own)
-    gain, w_in = held[:2]
+def fetch(stored, held, arrived, order):
     copies = [pltpu.make_async_copy(a, b, arrived.at[i]) for i, (a, b) in enumerate(zip(stored, held))]
-    for i in (2, 0, 1, *range(3, ARGS)):
+    for i in order:
         copies[i].start()
+    return copies
+
+
+def own_tokens_kernel(gain_in, w_in_in, own_in, inner, normed, gain, w_in, own, arrived, middle, scale):
+    copies = fetch((gain_in, w_in_in, own_in), (gain, w_in, own), arrived, (2, 0, 1))
     copies[2].wait()
     norm_tokens(own, normed, gain, middle, scale, copies[0])
     copies[1].wait()
     inner[...] = dot(normed[...], w_in[...]).astype(bf16)
-    for copy in copies[3:]:
-        copy.wait()
-
-
-def other_tokens_kernel(other, gain, w_in, inner_own, inner, tail, normed, middle, scale):
+
+
+def other_tokens_kernel(other, gain, w_in, inner_own, *refs):
+    stored, refs = refs[:LATER], refs[LATER:]
+    inner, tail, normed, *held = refs[: 3 + LATER]
+    arrived, middle, scale = refs[3 + LATER :]
+    copies = fetch(stored, held, arrived, range(LATER))
     half = other.shape[0]
     tp = lax.axis_index("tp")
     norm_tokens(other, normed, gain, middle, scale)
@@ -89,14 +87,16 @@
     there = pl.ds(pl.multiple_of((1 - tp) * half, half), half)
     inner[there, :] = dot(normed[...], w_in[...]).astype(bf16)
     tail[...] = inner[pl.ds(2 * half - 2 * HALO, 2 * HALO), :].astype(f32)[HALO:].astype(bf16)
-
-
-def gates(pre_r, pre_i, x, b_decay, b_input, rate, shift):
-    retain = sigmoid(pre_r + b_decay)
-    admit = sigmoid(pre_i + b_input)
-    loss = retain * (8.0 * rate) + shift
-    decay = jnp.exp(-loss)
-    rest = jnp.tanh(loss) * (1.0 + decay * decay)
+    for copy in copies:
+        copy.wait()
+
+
+def gates(minus_r, minus_i, x, b_decay, b_input, rate, shift):
+    retain = 1.0 / (1.0 + jnp.exp(minus_r - b_decay))
+    admit = 1.0 / (1.0 + jnp.exp(minus_i - b_input))
+    log_decay = retain * (-8.0 * rate) + shift
+    decay = jnp.exp(log_decay)
+    rest = jnp.tanh(log_decay) * (-1.0 - decay * decay)
     return decay, rest * lax.rsqrt(jnp.maximum(rest, 1e-37)) * admit * x
 
 
@@ -138,8 +138,8 @@
     blocks[...] = jnp.zeros_like(blocks)
     for head in range(heads):
         q, i = head // per, (head % per) * block
-        blocks[q, pl.ds(i, block), pl.ds(i, block)] = w_decay[head]
-        blocks[q, pl.ds(i, block), pl.ds(wide + i, block)] = w_input[head]
+        blocks[q, pl.ds(i, block), pl.ds(i, block)] = -w_decay[head]
+        blocks[q, pl.ds(i, block), pl.ds(wide + i, block)] = -w_input[head]
 
     def store(at, r, i):
         pre_r[:, at] = r
@@ -154,7 +154,7 @@
     moved = lax.dot_general(parts, order, (((1,), (1,)), ((), ())), preferred_element_type=f32).astype(bf16)
     r = lax.broadcasted_iota(jnp.int32, (4 * heads, width), 0)
     c = lax.broadcasted_iota(jnp.int32, (4 * heads, width), 1)
-    spread = jnp.where((r & (heads - 1)) == (c >> 6), -1.0, 0.0).astype(bf16)
+    spread = jnp.where((r & (heads - 1)) == (c >> 6), 1.0, 0.0).astype(bf16)
     shift[...] = lax.dot_general(moved, spread, (((0,), (0,)), ((), ())), preferred_element_type=f32)
     heads_shift[...] = shift[pl.ds(0, heads_shift.shape[0]), :]
 
@@ -187,7 +187,9 @@
         gate[at, :] = dot(normed[...], w_gate[...]).astype(bf16)
         for i in range(c * blocks_half, (c + 1) * blocks_half):
             h, p = scan_rows(i, (h, p), 0 if i else taps - 1)
-    g_out[...] = jax.nn.gelu(dot(order, gate[...]))
+    each = length // 4
+    for c in range(0, length, each):
+        g_out[c : c + each, :] = jax.nn.gelu(dot(order[c : c + each], gate[...]))
     ends_out[0] = p
     ends_out[1] = h
 
@@ -302,7 +304,7 @@
 
 
 HBM = pl.BlockSpec(memory_space=pltpu.HBM)
-ARGS = 11
+LATER = 8
 
 
 def call(kernel, inputs, out_shape, scratch=(), out_specs=None):
@@ -348,30 +350,30 @@
     other = lax.ppermute(tokens, "tp", swap)
 
     row = lambda v: v.reshape(1, -1)
-    fetched = (
-        row(norm_gain), in_weight, tokens, gate_weight,
-        conv_weight, decay_gate_weight, row(decay_gate_bias),
+    later = (
+        gate_weight, conv_weight, decay_gate_weight, row(decay_gate_bias),
         input_gate_weight, row(input_gate_bias), row(channel_decay_rate), forgetting_offset,
     )
     big = pltpu.VMEM
     like = lambda a: big(a.shape, a.dtype)
     square = big((length, width), f32)
     stats = [big((half, 128), f32), big((half, 128), f32)]
-    inner_own, normed_own, gain, w_in, *held = call(
+    gain = row(norm_gain)
+    inner_own, normed_own, gain, w_in = call(
         own_tokens_kernel,
-        (0, ARGS),
+        (0, 3),
+        (big((half, width), bf16), big((half, features), bf16), like(gain), like(in_weight)),
+        scratch=[like(tokens), pltpu.SemaphoreType.DMA((3,)), *stats],
+    )(gain, in_weight, tokens)
+    inner, tail, normed_other, *held = call(
+        other_tokens_kernel,
+        (4, LATER),
         (
-            big((half, width), bf16), big((half, features), bf16),
-            *(like(a) for i, a in enumerate(fetched) if i != 2),
+            big((length, width), bf16), big((HALO, width), bf16), big((half, features), bf16),
+            *(like(a) for a in later),
         ),
-        scratch=[like(tokens), pltpu.SemaphoreType.DMA((ARGS,)), *stats],
-    )(*fetched)
-    inner, tail, normed_other = call(
-        other_tokens_kernel,
-        (4, 0),
-        (big((length, width), bf16), big((HALO, width), bf16), big((half, features), bf16)),
-        scratch=stats,
-    )(other, gain, w_in, inner_own)
+        scratch=[pltpu.SemaphoreType.DMA((LATER,)), *stats],
+    )(other, gain, w_in, inner_own, *later)
     w_gate, conv, w_decay, b_decay, w_input, b_input, rate, offset = held
     halo = lax.ppermute(tail, SP, [(s, s + 1) for s in range(count - 1)])
     taps = conv_weight.shape[0]

time: 61.3 us -> 61.1 us (level)
  no operation moved by 1% of the time
where the time goes in v3:
time: 61.1 us; the launch traced here: 60.9 us
  blocking collectives  31.8 us (52%)
  starting transfers between devices  15.3 us (25%)
  Pallas kernels  12.3 us (20%)
  waiting for transfers between devices  1.34 us (2%)
    all_to_all x1, blocking collectives, step(): lax.all_to_all(sent, 'sp_0', split_axis=0, concat_axis=0, tiled=True)  16.7 us
    all_to_all x1, blocking collectives, step(): lax.all_to_all(sent, PLANE, split_axis=0, concat_axis=0, tiled=True)  15.1 us
    pallas_call x8, Pallas kernels, call(): return lambda *args: run(*(place(i, a) for i, a in enumerate(args)))  12.3 us
    ppermute x1, starting transfers between devices, step(): other = lax.ppermute(tokens, 'tp', swap)  8.73 us
    ppermute x1, starting transfers between devices, step(): received = lax.ppermute(theirs, 'tp', swap)  5.3 us
    ppermute x1, waiting for transfers between devices, step(): received = lax.ppermute(theirs, 'tp', swap)  1.34 us
    ppermute x1, starting transfers between devices, step(): halo = lax.ppermute(tail, SP, [(s, s + 1) for s in range(count - 1)])  1.29 us
  transfers between devices with their start and end apart: 3, of which 1 were waited for; matrix products, arithmetic and copies ran while one was open for 0% of the time, Pallas kernels for 13%

profile of v3, /device:TPU:1, one launch (start us, length us, event | category | flops | bytes accessed | tf_op | source)
XLA Modules:
  0.0 60.9 jit_solution(17416813714826812723)
XLA Ops:
  0.0 8.7 %collective-permute-start = (bf16[256,2048]{1,0:T(8,128)(2,1)}, bf16[256,2048]{1,0:T(8,128)(2,1)S(1)}, u32[]{:S(2)}, u32[]{:S(2)}) collective-permute-start(bf16[256,2048]{1,0:T(8,128)(2,1)} %own_in.1), channel_id=1, source_target_pairs={{0,1},{1,0},{2,3},{3,2},{4,5},{5,4},{6,7},{7,6},{8,9},{9,8},{10,11... | collective-permute-start | bytes 3145736 | tf_op jit(solution)/shard_map/ppermute | solution.py:350
  8.7 3.1 %shard_map.118 = (bf16[256,512]{1,0:T(8,128)(2,1)S(1)}, bf16[256,2048]{1,0:T(8,128)(2,1)S(1)}, f32[1,2048]{1,0:T(1,128)S(1)}, bf16[2048,512]{1,0:T(8,128)(2,1)S(1)}) custom-call(f32[1,2048]{1,0:T(1,128)} %bitcast.4, bf16[2048,512]{1,0:T(8,128)(2,1)} %w_in_in.1, bf16[256,2048]{1,0:T(8,128)(2,1)} %own_in.1), custom_call_target="tpu_custom_call" | custom-call | tf_op jit(solution)/shard_map/pallas_call | solution.py:323
  11.8 0.0 collective-permute-done.other
  11.9 2.0 %shard_map.119 = (bf16[512,512]{1,0:T(8,128)(2,1)S(1)}, bf16[8,512]{1,0:T(8,128)(2,1)S(1)}, bf16[256,2048]{1,0:T(8,128)(2,1)S(1)}, bf16[2048,512]{1,0:T(8,128)(2...) custom-call(bf16[256,2048]{1,0:T(8,128)(2,1)S(1)} %collective-permut, ...), custom_call_target="tpu_custom_call" | custom-call | tf_op jit(solution)/shard_map/pallas_call | solution.py:323
  13.9 1.3 %collective-permute-start.1 = (bf16[8,512]{1,0:T(8,128)(2,1)S(1)}, bf16[8,512]{1,0:T(8,128)(2,1)S(1)}, u32[]{:S(2)}, u32[]{:S(2)}) collective-permute-start(bf16[8,512]{1,0:T(8,128)(2,1)S(1)} %get-tuple-element.37), channel_id=1, source_target_pairs={{0,2},{2,4},{4,6},{6,8},{8,10},{10,12},{12,14},{14,16},{16,18},{18... | collective-permute-start | bytes 24584 | tf_op jit(solution)/shard_map/ppermute | solution.py:378
  15.2 0.0 copy-start
  15.2 3.7 %shard_map.120 = (f32[512,512]{1,0:T(8,128)S(1)}, f32[512,512]{1,0:T(8,128)S(1)}, f32[512,512]{1,0:T(8,128)S(1)}, f32[2,8,512]{2,1,0:T(8,128)S(1)}, bf16[2,256,5...) custom-call(bf16[512,512]{1,0:T(8,128)(2,1)S(1)} %get-tuple-element.36.inner, ...), custom_call_target="tpu_custom_call" | custom-call | tf_op jit(solution)/shard_map/pallas_call | solution.py:323
  18.9 0.0 collective-permute-done.1.halo
  18.9 0.3 shard_map.121
  19.2 15.1 %all_to_all.10.pieces = f32[32,2,512]{2,1,0:T(2,128)S(1)} all-to-all(f32[32,2,512]{2,1,0:T(2,128)S(1)} %get-tuple-element.51), channel_id=1, replica_groups=mesh['sp_0'=8,'sp_1'=8,'sp_2'=4,'tp'=2] {'sp_1','sp_2'}, dimensions={0} | all-to-all | bytes 262144 | tf_op jit(solution)/shard_map/all_to_all | solution.py:401
  34.3 0.1 shard_map.122
  34.4 16.7 %all_to_all.11.pieces = f32[8,2,512]{2,1,0:T(2,128)S(1)} all-to-all(f32[8,2,512]{2,1,0:T(2,128)S(1)} %get-tuple-element.52), channel_id=1, replica_groups=mesh['sp_0'=8,'sp_1'=8,'sp_2'=4,'tp'=2] {'sp_0'}, dimensions={0} | all-to-all | bytes 65536 | tf_op jit(solution)/shard_map/all_to_all | solution.py:403
  51.1 0.0 copy-done
  51.1 1.2 %shard_map.123 = (bf16[512,512]{1,0:T(8,128)(2,1)S(1)}, bf16[256,2048]{1,0:T(8,128)(2,1)S(1)}) custom-call(f32[8,2,512]{2,1,0:T(2,128)S(1)} %all_to_all.11.pieces, f32[2,512]{1,0:T(2,128)S(1)} %get-tuple-element.53.before, f32[2,8,512]{2,1,0:T(8,128)S(1)} %get-tuple-element.54.runs, f32[2,3,512]{2,1,0:T(4,128)S(1)} %get-tuple-element.55.heads, ...), custom_call_target="tpu_custom_call" | custom-call | tf_op jit(solution)/shard_map/pallas_call | solution.py:323
  52.3 5.3 %collective-permute-start.2 = (bf16[256,2048]{1,0:T(8,128)(2,1)S(1)}, bf16[256,2048]{1,0:T(8,128)(2,1)S(1)}, u32[]{:S(2)}, u32[]{:S(2)}) collective-permute-start(bf16[256,2048]{1,0:T(8,128)(2,1)S(1)} %get-tuple-element.60), channel_id=1, source_target_pairs={{0,1},{1,0},{2,3},{3,2},{4,5},{5,4},{6,7},{7,6},{8,9},{9,8},{10,11... | collective-permute-start | bytes 3145736 | tf_op jit(solution)/shard_map/ppermute | solution.py:407
  57.6 0.9 %shard_map.124.part = f32[256,2048]{1,0:T(8,128)S(1)} custom-call(bf16[512,512]{1,0:T(8,128)(2,1)S(1)} %get-tuple-element.59.gated, bf16[512,2048]{1,0:T(8,128)(2,1)S(1)} %copy-done), custom_call_target="tpu_custom_call" | custom-call | tf_op jit(solution)/shard_map/pallas_call | solution.py:323
  58.5 1.3 %collective-permute-done.2.received = bf16[256,2048]{1,0:T(8,128)(2,1)S(1)} collective-permute-done((bf16[256,2048]{1,0:T(8,128)(2,1)S(1)}, bf16[256,2048]{1,0:T(8,128)(2,1)S(1)}, u32[]{:S(2)}, u32[]{:S(2)}) %collective-permute-start.2) | collective-permute-done | bytes 1048608 | tf_op jit(solution)/shard_map/ppermute | solution.py:407
  59.9 1.0 %shard_map.125 = bf16[256,2048]{1,0:T(8,128)(2,1)} custom-call(f32[256,2048]{1,0:T(8,128)S(1)} %shard_map.124.part, bf16[256,2048]{1,0:T(8,128)(2,1)S(1)} %collective-permute-done.2.received), custom_call_target="tpu_custom_call" | custom-call | tf_op jit(solution)/shard_map/pallas_call | solution.py:323
Async XLA Ops:
  0.0 11.8 %collective-permute-start = (bf16[256,2048]{1,0:T(8,128)(2,1)}, bf16[256,2048]{1,0:T(8,128)(2,1)S(1)}, u32[]{:S(2)}, u32[]{:S(2)}) collective-permute-start(bf16[256,2048]{1,0:T(8,128)(2,1)} %own_in.1), channel_id=1, source_target_pairs={{0,1},{1,0},{2,3},{3,2},{4,5},{5,4},{6,7},{7,6},{8,9},{9,8},{10,11... | collective-permute-start | bytes 3145736 | tf_op jit(solution)/shard_map/ppermute | solution.py:350
  13.9 5.1 %collective-permute-start.1 = (bf16[8,512]{1,0:T(8,128)(2,1)S(1)}, bf16[8,512]{1,0:T(8,128)(2,1)S(1)}, u32[]{:S(2)}, u32[]{:S(2)}) collective-permute-start(bf16[8,512]{1,0:T(8,128)(2,1)S(1)} %get-tuple-element.37), channel_id=1, source_target_pairs={{0,2},{2,4},{4,6},{6,8},{8,10},{10,12},{12,14},{14,16},{16,18},{18... | collective-permute-start | bytes 24584 | tf_op jit(solution)/shard_map/ppermute | solution.py:378
  15.2 35.9 %copy-start = (bf16[512,2048]{1,0:T(8,128)(2,1)S(1)}, bf16[512,2048]{1,0:T(8,128)(2,1)}, u32[]{:S(2)}) copy-start(bf16[512,2048]{1,0:T(8,128)(2,1)} %w_mine.3) | copy-start | bytes 6291460
  52.3 7.6 %collective-permute-start.2 = (bf16[256,2048]{1,0:T(8,128)(2,1)S(1)}, bf16[256,2048]{1,0:T(8,128)(2,1)S(1)}, u32[]{:S(2)}, u32[]{:S(2)}) collective-permute-start(bf16[256,2048]{1,0:T(8,128)(2,1)S(1)} %get-tuple-element.60), channel_id=1, source_target_pairs={{0,1},{1,0},{2,3},{3,2},{4,5},{5,4},{6,7},{7,6},{8,9},{9,8},{10,11... | collective-permute-start | bytes 3145736 | tf_op jit(solution)/shard_map/ppermute | solution.py:407

commit v4 on v3

--- a/solution.py
+++ b/solution.py
@@ -194,13 +194,23 @@
     ends_out[1] = h
 
 
-def head_kernel(
-    inner, halo, conv, blocks, b_decay, b_input, rate, shift, ends,
-    runs_out, heads_out, sent_out,
-    near, smoothed, pre_r, pre_i,
+def pack_kernel(
+    inner, halo, conv, blocks, b_decay, b_input, rate, shift, ends, h, p, g, weight,
+    runs_out, mine_out, packed_out, sent_out,
+    near, smoothed, pre_r, pre_i, gated_h, gated_p, arrived,
 ):
-    width = inner.shape[1]
+    length, width = inner.shape
+    half, run = length // 2, length // SUB
     taps = conv.shape[0]
+    cols = weight.shape[1] // width
+    copies = [
+        pltpu.make_async_copy(
+            weight.at[:, pl.ds(q * width, width)], packed_out.at[pl.ds((q + 1) * width, width)], arrived.at[q]
+        )
+        for q in range(cols)
+    ]
+    for copy in copies:
+        copy.start()
     near[pl.ds(0, HALO), :] = halo[...].astype(f32)
     near[pl.ds(HALO, HALO), :] = inner[pl.ds(0, 2 * HALO), :].astype(f32)[:HALO]
     smooth = near[pl.ds(HALO - taps + 1, HALO), :] * conv[0:1, :]
@@ -217,85 +227,118 @@
     decay, drive = gates(
         pre_r[...], pre_i[...], smoothed[...].astype(f32)[:HALO], b_decay[...], b_input[...], rate[...], shifts
     )
-    a_before, b_before = jnp.ones((1, width), f32), jnp.zeros((1, width), f32)
+    one, zero = jnp.ones((1, width), f32), jnp.zeros((1, width), f32)
+    a_head, b_head, opening = one, zero, []
     for k in range(taps - 1):
         a_k = decay[k : k + 1, :]
-        a_before, b_before = a_before * a_k, a_k * b_before + drive[k : k + 1, :]
-        heads_out[0, k : k + 1, :] = a_before
-        heads_out[1, k : k + 1, :] = b_before
+        a_head, b_head = a_head * a_k, a_k * b_head + drive[k : k + 1, :]
+        opening.append((a_head, b_head))
+    runs_a, runs_b = [one], [zero]
+    a_before, b_before = a_head, b_head
     for s in range(SUB):
-        runs_out[0, s : s + 1, :] = a_before
-        runs_out[1, s : s + 1, :] = b_before
         a_s = ends[0, s : s + 1, :]
         a_before, b_before = a_before * a_s, a_s * b_before + ends[1, s : s + 1, :]
+        runs_a.append(a_before)
+        runs_b.append(b_before)
     pair = jnp.concatenate([a_before, b_before], axis=0)
     sent_out[...] = jnp.broadcast_to(pair[None], sent_out.shape)
+    runs = jnp.concatenate(runs_a[:SUB] + runs_b[:SUB], axis=0)
+    runs_out[...] = runs
+
+    first = lax.broadcasted_iota(jnp.int32, (SUB, width), 0) == 0
+    times = jnp.where(first, a_head, 1.0)
+    plus = jnp.where(first, b_head, 0.0)
+    rows = 4 * SUB
+    times, plus = (jnp.concatenate([v] * (rows // SUB), axis=0) for v in (times, plus))
+
+    def gate_rows(i, patch=False):
+        at = pl.ds(pl.multiple_of(i * rows, rows), rows)
+        ph, pp, pg = h[at, :], p[at, :], g[at, :]
+        ph, pp = ph + pp * plus, pp * times
+        if patch:
+            r = lax.broadcasted_iota(jnp.int32, (rows, width), 0)
+            for k, (a_k, b_k) in enumerate(opening):
+                ph, pp = jnp.where(r == k * SUB, b_k, ph), jnp.where(r == k * SUB, a_k, pp)
+        gated_h[at, :] = (ph * pg).astype(bf16)
+        gated_p[at, :] = (pp * pg).astype(bf16)
+
+    gate_rows(0, True)
+    lax.fori_loop(1, length // rows, lambda i, _: (gate_rows(i), 0)[1], 0)
+
+    def back(gated, begin):
+        t = lax.broadcasted_iota(jnp.int32, (half, length), 0) + begin
+        c = lax.broadcasted_iota(jnp.int32, (half, length), 1)
+        pick = jnp.where(t == (c & (SUB - 1)) * run + (c >> 3), 1.0, 0.0).astype(bf16)
+        return dot(pick, gated[...]).astype(bf16)
+
+    tp = lax.axis_index("tp")
+    for i, gated in enumerate((gated_h, gated_p)):
+        packed_out[pl.ds(i * half, half), :] = back(gated, (1 - tp) * half)
+        mine_out[pl.ds(i * half, half), :] = back(gated, tp * half)
+    rest = runs
+    for i in range(PARTS):
+        part = rest.astype(bf16)
+        packed_out[pl.ds((cols + 1) * width + i * 2 * SUB, 2 * SUB), :] = part
+        rest = rest - part.astype(f32)
+    for copy in copies:
+        copy.wait()
 
 
 def before_in(pieces, index):
-    width = pieces.shape[2]
+    width = pieces[0].shape[1]
     a, b = jnp.ones((1, width), f32), jnp.zeros((1, width), f32)
     a_at, b_at = a, b
-    for k in range(pieces.shape[0]):
+    for k, piece in enumerate(pieces):
         here = k == index
         a_at, b_at = jnp.where(here, a, a_at), jnp.where(here, b, b_at)
-        a_k, b_k = pieces[k, 0:1, :], pieces[k, 1:2, :]
+        a_k, b_k = piece[0:1], piece[1:2]
         a, b = a * a_k, a_k * b + b_k
     return (a_at, b_at), (a, b)
 
 
 def plane_kernel(pieces, before_out, sent_out):
     index = lax.axis_index("sp_1") * lax.axis_size("sp_2") + lax.axis_index("sp_2")
-    (a_at, b_at), (a, b) = before_in(pieces, index)
-    before_out[...] = jnp.concatenate([a_at, b_at], axis=0)
+    (a_at, b_at), (a, b) = before_in([pieces[k] for k in range(pieces.shape[0])], index)
+    before = jnp.concatenate([a_at, b_at], axis=0)
+    before_out[...] = before
     pair = jnp.concatenate([a, b], axis=0)
-    sent_out[...] = jnp.broadcast_to(pair[None], sent_out.shape)
-
-
-def back(gated, first):
-    length = gated.shape[0]
-    half, run = length // 2, length // SUB
-    t = lax.broadcasted_iota(jnp.int32, (half, length), 0) + first
-    c = lax.broadcasted_iota(jnp.int32, (half, length), 1)
-    pick = jnp.where(t == (c & (SUB - 1)) * run + (c >> 3), 1.0, 0.0).astype(bf16)
-    return dot(pick, gated[...]).astype(bf16)
-
-
-def state_kernel(pieces, before, runs, heads, h, p, g, w_mine, gated, theirs_out):
-    (_, b_at), _ = before_in(pieces, lax.axis_index("sp_0"))
-    carried = before[0:1, :] * b_at + before[1:2, :]
-    start = runs[0] * carried + runs[1]
-    length = h.shape[0]
-    rows = 4 * SUB
-    opening = heads[0] * carried + heads[1]
-    first = [jnp.concatenate([opening[k : k + 1], start[1:]], axis=0) for k in range(heads.shape[1])]
-    groups = rows // SUB
-
-    def state_rows(i, starts):
-        at = pl.ds(pl.multiple_of(i * rows, rows), rows)
-        gated[at, :] = ((h[at, :] + p[at, :] * starts) * g[at, :]).astype(bf16)
-        return starts
-
-    state_rows(0, jnp.concatenate(first + [start] * (groups - len(first)), axis=0))
-    starts = jnp.concatenate([start] * groups, axis=0)
-    lax.fori_loop(1, length // rows, lambda i, _: (state_rows(i, starts), 0)[1], 0)
-    theirs = back(gated, (1 - lax.axis_index("tp")) * (length // 2))
-    theirs_out[...] = dot(theirs, w_mine[...]).astype(bf16)
-
-
-def own_kernel(gated, w_mine, part):
-    mine = back(gated, lax.axis_index("tp") * (gated.shape[0] // 2))
-    part[...] = dot(mine, w_mine[...])
-
-
-def out_kernel(part, received, out, block, sent):
-    rows = block.shape[1]
+    partner = lax.axis_index("sp_0") * 2 + 1 - lax.axis_index("tp")
+    for k in range(sent_out.shape[0]):
+        sent_out[k] = jnp.where(k == partner, before, pair)
+
+
+def out_kernel(pieces, before, runs, mine, packed, received, out, theirs, block, gated_mine, gated_theirs, sent):
+    half, width = out.shape[0], mine.shape[1]
+    run = half // (SUB // 2)
+    deep = pieces.shape[0] // 2
+    at, tp = lax.axis_index("sp_0"), lax.axis_index("tp")
+    is_one = tp == 1
+    for k in range(deep):
+        theirs[k] = jnp.where(is_one, pieces[2 * k], pieces[2 * k + 1])
+    own = [jnp.where(is_one, pieces[2 * k + 1], pieces[2 * k]) for k in range(deep)]
+    cols = out.shape[1] // width
+    last = (cols + 1) * width
+    their_runs = sum(received[pl.ds(last + i * 2 * SUB, 2 * SUB), :].astype(f32) for i in range(PARTS))
+    sides = (
+        (own, before[...], runs[...], mine, gated_mine),
+        ([theirs[k] for k in range(deep)], theirs[at], their_runs, received, gated_theirs),
+    )
+    for totals, near, steps, parts, gated in sides:
+        (_, b_at), _ = before_in(totals, at)
+        carried = near[0:1] * b_at + near[1:2]
+        start = steps[:SUB] * carried + steps[SUB:]
+        start = jnp.where(is_one, start[SUB // 2 :], start[: SUB // 2])
+        for u in range(SUB // 2):
+            here, there = pl.ds(u * run, run), pl.ds(half + u * run, run)
+            gated[here, :] = (
+                parts[here, :].astype(f32) + parts[there, :].astype(f32) * start[u : u + 1]
+            ).astype(bf16)
     copies = []
-    for i in range(block.shape[0]):
-        at = pl.ds(i * rows, rows)
-        block[i] = (part[at, :] + received[at, :].astype(f32)).astype(bf16)
-        copies.append(pltpu.make_async_copy(block.at[i], out.at[at, :], sent.at[i]))
-        copies[i].start()
+    for q in range(cols):
+        w = pl.ds((q + 1) * width, width)
+        block[q] = (dot(gated_mine[...], packed[w, :]) + dot(gated_theirs[...], received[w, :])).astype(bf16)
+        copies.append(pltpu.make_async_copy(block.at[q], out.at[:, pl.ds(q * width, width)], sent.at[q]))
+        copies[q].start()
     for copy in copies:
         copy.wait()
 
@@ -304,6 +347,7 @@
 
 
 HBM = pl.BlockSpec(memory_space=pltpu.HBM)
+PARTS = 3
 LATER = 8
 
 
@@ -389,31 +433,36 @@
             big((length + (taps - 1) * SUB, width), f32), big((length, width), bf16),
         ],
     )(inner, normed_own, normed_other, w_gate, conv, w_decay, b_decay, w_input, b_input, rate, offset)
-    runs, opening, sent = call(
-        head_kernel,
-        (9, 0),
-        (big((2, SUB, width), f32), big((2, taps - 1, width), f32), big((plane, 2, width), f32)),
+    cols = features // width
+    packed_rows = (cols + 1) * width + PARTS * 2 * SUB
+    runs, mine, packed, sent = call(
+        pack_kernel,
+        (12, 1),
+        (
+            big((2 * SUB, width), f32), big((length, width), bf16),
+            big((packed_rows, width), bf16), big((plane, 2, width), f32),
+        ),
         scratch=[
             big((2 * HALO, width), f32), big((2 * HALO, width), bf16),
             big((HALO, width), f32), big((HALO, width), f32),
+            big((length, width), bf16), big((length, width), bf16),
+            pltpu.SemaphoreType.DMA((cols,)),
         ],
-    )(inner, halo, conv, blocks, b_decay, b_input, rate, shift, ends)
+    )(inner, halo, conv, blocks, b_decay, b_input, rate, shift, ends, h, p, g, out_weight)
+    received = lax.ppermute(packed, "tp", swap)
     pieces = lax.all_to_all(sent, PLANE, split_axis=0, concat_axis=0, tiled=True)
-    before, sent = call(plane_kernel, (1, 0), (big((2, width), f32), big((deep, 2, width), f32)))(pieces)
-    pieces = lax.all_to_all(sent, "sp_0", split_axis=0, concat_axis=0, tiled=True)
-    gated, theirs = call(
-        state_kernel, (8, 0), (big((length, width), bf16), big((half, features), bf16))
-    )(pieces, before, runs, opening, h, p, g, out_weight)
-    received = lax.ppermute(theirs, "tp", swap)
-    part = call(own_kernel, (2, 0), big((half, features), f32))(gated, out_weight)
-    rows = 64
+    before, sent = call(plane_kernel, (1, 0), (big((2, width), f32), big((2 * deep, 2, width), f32)))(pieces)
+    pieces = lax.all_to_all(sent, ("sp_0", "tp"), split_axis=0, concat_axis=0, tiled=True)
     return call(
         out_kernel,
-        (2, 0),
+        (6, 0),
         S((half, features), bf16),
-        scratch=(big((half // rows, rows, features), bf16), pltpu.SemaphoreType.DMA((half // rows,))),
+        scratch=(
+            big((deep, 2, width), f32), big((cols, half, width), bf16),
+            big((half, width), bf16), big((half, width), bf16), pltpu.SemaphoreType.DMA((cols,)),
+        ),
         out_specs=HBM,
-    )(part, received)
+    )(pieces, before, runs, mine, packed, received)
 
 
 def solution(mesh):

time: 61.1 us -> 60.1 us (0.984)
  blocking collectives: 31.8 us -> 35.2 us
  starting transfers between devices: 15.3 us -> 11.9 us
  waiting for transfers between devices: 1.34 us -> 0.01 us
    ppermute x1, starting transfers between devices: 5.3 us -> 1.92 us  [step(): received = lax.ppermute(packed, 'tp', swap)]
    all_to_all x1, blocking collectives: 16.7 us -> 19.8 us  [step(): lax.all_to_all(sent, ('sp_0', 'tp'), split_axis=0, concat_axis=0, tiled=T...]
    ppermute x1, waiting for transfers between devices: 1.34 us -> 0.01 us  [step(): received = lax.ppermute(packed, 'tp', swap)]
    pallas_call x8 -> x6, Pallas kernels: 12.3 us -> 12.6 us  [call(): return lambda *args: run(*(place(i, a) for i, a in enumerate(args)))]
  transfers between devices with their start and end apart: 3 -> 3, of which waited for: 1 -> 0; matrix products, arithmetic and copies ran while one was open for 0% -> 0% of each run, Pallas kernels for 13% -> 12%
where the time goes in v4:
time: 60.1 us; the launch traced here: 59.8 us
  blocking collectives  35.2 us (59%)
  Pallas kernels  12.6 us (21%)
  starting transfers between devices  11.9 us (20%)
    all_to_all x1, blocking collectives, step(): lax.all_to_all(sent, ('sp_0', 'tp'), split_axis=0, concat_axis=0, tiled=T...  19.8 us
    all_to_all x1, blocking collectives, step(): lax.all_to_all(sent, PLANE, split_axis=0, concat_axis=0, tiled=True)  15.4 us
    pallas_call x6, Pallas kernels, call(): return lambda *args: run(*(place(i, a) for i, a in enumerate(args)))  12.6 us
    ppermute x1, starting transfers between devices, step(): other = lax.ppermute(tokens, 'tp', swap)  8.73 us
    ppermute x1, starting transfers between devices, step(): received = lax.ppermute(packed, 'tp', swap)  1.92 us
    ppermute x1, starting transfers between devices, step(): halo = lax.ppermute(tail, SP, [(s, s + 1) for s in range(count - 1)])  1.29 us
  transfers between devices with their start and end apart: 3, of which 0 were waited for; matrix products, arithmetic and copies ran while one was open for 0% of the time, Pallas kernels for 12%

profile of v4, /device:TPU:1, one launch (start us, length us, event | category | flops | bytes accessed | tf_op | source)
XLA Modules:
  0.0 59.8 jit_solution(3614648840354382307)
XLA Ops:
  0.0 8.7 %collective-permute-start = (bf16[256,2048]{1,0:T(8,128)(2,1)}, bf16[256,2048]{1,0:T(8,128)(2,1)S(1)}, u32[]{:S(2)}, u32[]{:S(2)}) collective-permute-start(bf16[256,2048]{1,0:T(8,128)(2,1)} %own_in.1), channel_id=1, source_target_pairs={{0,1},{1,0},{2,3},{3,2},{4,5},{5,4},{6,7},{7,6},{8,9},{9,8},{10,11... | collective-permute-start | bytes 3145736 | tf_op jit(solution)/shard_map/ppermute | solution.py:394
  8.7 3.1 %shard_map.118 = (bf16[256,512]{1,0:T(8,128)(2,1)S(1)}, bf16[256,2048]{1,0:T(8,128)(2,1)S(1)}, f32[1,2048]{1,0:T(1,128)S(1)}, bf16[2048,512]{1,0:T(8,128)(2,1)S(1)}) custom-call(f32[1,2048]{1,0:T(1,128)} %bitcast.4, bf16[2048,512]{1,0:T(8,128)(2,1)} %w_in_in.1, bf16[256,2048]{1,0:T(8,128)(2,1)} %own_in.1), custom_call_target="tpu_custom_call" | custom-call | tf_op jit(solution)/shard_map/pallas_call | solution.py:367
  11.8 0.0 collective-permute-done.other
  11.9 2.0 %shard_map.119 = (bf16[512,512]{1,0:T(8,128)(2,1)S(1)}, bf16[8,512]{1,0:T(8,128)(2,1)S(1)}, bf16[256,2048]{1,0:T(8,128)(2,1)S(1)}, bf16[2048,512]{1,0:T(8,128)(2...) custom-call(bf16[256,2048]{1,0:T(8,128)(2,1)S(1)} %collective-permut, ...), custom_call_target="tpu_custom_call" | custom-call | tf_op jit(solution)/shard_map/pallas_call | solution.py:367
  13.9 1.3 %collective-permute-start.1 = (bf16[8,512]{1,0:T(8,128)(2,1)S(1)}, bf16[8,512]{1,0:T(8,128)(2,1)S(1)}, u32[]{:S(2)}, u32[]{:S(2)}) collective-permute-start(bf16[8,512]{1,0:T(8,128)(2,1)S(1)} %get-tuple-element.36), channel_id=1, source_target_pairs={{0,2},{2,4},{4,6},{6,8},{8,10},{10,12},{12,14},{14,16},{16,18},{18... | collective-permute-start | bytes 24584 | tf_op jit(solution)/shard_map/ppermute | solution.py:422
  15.2 3.7 %shard_map.120 = (f32[512,512]{1,0:T(8,128)S(1)}, f32[512,512]{1,0:T(8,128)S(1)}, f32[512,512]{1,0:T(8,128)S(1)}, f32[2,8,512]{2,1,0:T(8,128)S(1)}, bf16[2,256,5...) custom-call(bf16[512,512]{1,0:T(8,128)(2,1)S(1)} %get-tuple-element.35.inner, ...), custom_call_target="tpu_custom_call" | custom-call | tf_op jit(solution)/shard_map/pallas_call | solution.py:367
  18.9 0.0 collective-permute-done.1.halo
  18.9 1.6 %shard_map.121 = (f32[16,512]{1,0:T(8,128)S(1)}, bf16[512,512]{1,0:T(8,128)(2,1)S(1)}, bf16[2608,512]{1,0:T(8,128)(2,1)S(1)}, f32[32,2,512]{2,1,0:T(2,128)S(1)}) custom-call(bf16[512,512]{1,0:T(8,128)(2,1)S(1)} %get-tuple-element.35.inner, bf16[8,512]{1,0:T(8,128)(2,1)S(1)} %collective-permute-done.1.halo, f32[4,512]{1,0:T(4,128)S(1)} %get-tuple-element.37.conv, ...), custom_call_target="tpu_custom_call" | custom-call | tf_op jit(solution)/shard_map/pallas_call | solution.py:367
  20.5 1.9 %collective-permute-start.2 = (bf16[2608,512]{1,0:T(8,128)(2,1)S(1)}, bf16[2608,512]{1,0:T(8,128)(2,1)S(1)}, u32[]{:S(2)}, u32[]{:S(2)}) collective-permute-start(bf16[2608,512]{1,0:T(8,128)(2,1)S(1)} %get-tuple-element.58.packed), channel_id=1, source_target_pairs={{0,1},{1,0},{2,3},{3,2},{4,5},{5,4},{6,7},{7,6},{8,9},{9,8},{10,11... | collective-permute-start | bytes 8011784 | tf_op jit(solution)/shard_map/ppermute | solution.py:452
  22.5 15.4 %all_to_all.10.pieces = f32[32,2,512]{2,1,0:T(2,128)S(1)} all-to-all(f32[32,2,512]{2,1,0:T(2,128)S(1)} %get-tuple-element.53), channel_id=1, replica_groups=mesh['sp_0'=8,'sp_1'=8,'sp_2'=4,'tp'=2] {'sp_1','sp_2'}, dimensions={0} | all-to-all | bytes 262144 | tf_op jit(solution)/shard_map/all_to_all | solution.py:453
  37.8 0.1 shard_map.122
  37.9 19.8 %all_to_all.11.pieces = f32[16,2,512]{2,1,0:T(2,128)S(1)} all-to-all(f32[16,2,512]{2,1,0:T(2,128)S(1)} %get-tuple-element.54), channel_id=1, replica_groups=mesh['sp_0'=8,'sp_1'=8,'sp_2'=4,'tp'=2] {'sp_0','tp'}, dimensions={0} | all-to-all | bytes 131072 | tf_op jit(solution)/shard_map/all_to_all | solution.py:455
  57.8 0.0 collective-permute-done.2.received
  57.8 2.1 %shard_map.123 = bf16[256,2048]{1,0:T(8,128)(2,1)} custom-call(f32[16,2,512]{2,1,0:T(2,128)S(1)} %all_to_all.11.pieces, f32[2,512]{1,0:T(2,128)S(1)} %get-tuple-element.55.before, f32[16,512]{1,0:T(8,128)S(1)} %get-tuple-element.56.runs, bf16[512,512]{1,0:T(8,128)(2,1)S(1)} %get-tuple-element.57.mine, bf16[2608,512]{1,0:T(8,128)(2,1)S(1)} %get-tuple-element.58.packed, ...), custom_call_target="tpu_custom_call" | custom-call | tf_op jit(solution)/shard_map/pallas_call | solution.py:367
Async XLA Ops:
  0.0 11.8 %collective-permute-start = (bf16[256,2048]{1,0:T(8,128)(2,1)}, bf16[256,2048]{1,0:T(8,128)(2,1)S(1)}, u32[]{:S(2)}, u32[]{:S(2)}) collective-permute-start(bf16[256,2048]{1,0:T(8,128)(2,1)} %own_in.1), channel_id=1, source_target_pairs={{0,1},{1,0},{2,3},{3,2},{4,5},{5,4},{6,7},{7,6},{8,9},{9,8},{10,11... | collective-permute-start | bytes 3145736 | tf_op jit(solution)/shard_map/ppermute | solution.py:394
  13.9 5.0 %collective-permute-start.1 = (bf16[8,512]{1,0:T(8,128)(2,1)S(1)}, bf16[8,512]{1,0:T(8,128)(2,1)S(1)}, u32[]{:S(2)}, u32[]{:S(2)}) collective-permute-start(bf16[8,512]{1,0:T(8,128)(2,1)S(1)} %get-tuple-element.36), channel_id=1, source_target_pairs={{0,2},{2,4},{4,6},{6,8},{8,10},{10,12},{12,14},{14,16},{16,18},{18... | collective-permute-start | bytes 24584 | tf_op jit(solution)/shard_map/ppermute | solution.py:422
  20.5 37.2 %collective-permute-start.2 = (bf16[2608,512]{1,0:T(8,128)(2,1)S(1)}, bf16[2608,512]{1,0:T(8,128)(2,1)S(1)}, u32[]{:S(2)}, u32[]{:S(2)}) collective-permute-start(bf16[2608,512]{1,0:T(8,128)(2,1)S(1)} %get-tuple-element.58.packed), channel_id=1, source_target_pairs={{0,1},{1,0},{2,3},{3,2},{4,5},{5,4},{6,7},{7,6},{8,9},{9,8},{10,11... | collective-permute-start | bytes 8011784 | tf_op jit(solution)/shard_map/ppermute | solution.py:452

commit v5 on v4

--- a/solution.py
+++ b/solution.py
@@ -109,12 +109,20 @@
 
 
 def scan_kernel(
-    inner, normed_own, normed_other, w_gate, conv, w_decay, b_decay, w_input, b_input, rate, offset,
-    h_out, p_out, g_out, ends_out, blocks, heads_shift,
-    smoothed, pre_r, pre_i, shift, extended, gate,
+    inner, normed_own, normed_other, w_gate, conv, w_decay, b_decay, w_input, b_input, rate, offset, weight,
+    mine_out, packed_out, ends_out, blocks, heads_shift,
+    smoothed, pre_r, pre_i, shift, extended, gate, h_out, p_out, gated_h, gated_p, arrived,
 ):
     length, width = inner.shape
     run = length // SUB
+    copies = [
+        pltpu.make_async_copy(
+            weight.at[:, pl.ds(q * width, width)], packed_out.at[pl.ds((q + 1) * width, width)], arrived.at[q]
+        )
+        for q in range(weight.shape[1] // width)
+    ]
+    for copy in copies:
+        copy.start()
     taps = conv.shape[0]
     lead = (taps - 1) * SUB
 
@@ -189,28 +197,33 @@
             h, p = scan_rows(i, (h, p), 0 if i else taps - 1)
     each = length // 4
     for c in range(0, length, each):
-        g_out[c : c + each, :] = jax.nn.gelu(dot(order[c : c + each], gate[...]))
+        here = slice(c, c + each)
+        g = jax.nn.gelu(dot(order[here], gate[...]))
+        gated_h[here, :] = (h_out[here, :] * g).astype(bf16)
+        gated_p[here, :] = (p_out[here, :] * g).astype(bf16)
+
+    def back(gated, begin):
+        t = lax.broadcasted_iota(jnp.int32, (half, length), 0) + begin
+        c = lax.broadcasted_iota(jnp.int32, (half, length), 1)
+        pick = jnp.where(t == (c & (SUB - 1)) * run + (c >> 3), 1.0, 0.0).astype(bf16)
+        return dot(pick, gated[...]).astype(bf16)
+
+    for i, gated in enumerate((gated_h, gated_p)):
+        packed_out[pl.ds(i * half, half), :] = back(gated, (1 - tp) * half)
+        mine_out[pl.ds(i * half, half), :] = back(gated, tp * half)
+    for copy in copies:
+        copy.wait()
     ends_out[0] = p
     ends_out[1] = h
 
 
 def pack_kernel(
-    inner, halo, conv, blocks, b_decay, b_input, rate, shift, ends, h, p, g, weight,
-    runs_out, mine_out, packed_out, sent_out,
-    near, smoothed, pre_r, pre_i, gated_h, gated_p, arrived,
+    inner, halo, conv, blocks, b_decay, b_input, rate, shift, ends, packed,
+    small_out, packed_out, sent_out,
+    near, smoothed, pre_r, pre_i,
 ):
-    length, width = inner.shape
-    half, run = length // 2, length // SUB
+    width = inner.shape[1]
     taps = conv.shape[0]
-    cols = weight.shape[1] // width
-    copies = [
-        pltpu.make_async_copy(
-            weight.at[:, pl.ds(q * width, width)], packed_out.at[pl.ds((q + 1) * width, width)], arrived.at[q]
-        )
-        for q in range(cols)
-    ]
-    for copy in copies:
-        copy.start()
     near[pl.ds(0, HALO), :] = halo[...].astype(f32)
     near[pl.ds(HALO, HALO), :] = inner[pl.ds(0, 2 * HALO), :].astype(f32)[:HALO]
     smooth = near[pl.ds(HALO - taps + 1, HALO), :] * conv[0:1, :]
@@ -228,60 +241,27 @@
         pre_r[...], pre_i[...], smoothed[...].astype(f32)[:HALO], b_decay[...], b_input[...], rate[...], shifts
     )
     one, zero = jnp.ones((1, width), f32), jnp.zeros((1, width), f32)
-    a_head, b_head, opening = one, zero, []
+    a_before, b_before, head_a, head_b = one, zero, [], []
     for k in range(taps - 1):
         a_k = decay[k : k + 1, :]
-        a_head, b_head = a_head * a_k, a_k * b_head + drive[k : k + 1, :]
-        opening.append((a_head, b_head))
-    runs_a, runs_b = [one], [zero]
-    a_before, b_before = a_head, b_head
+        a_before, b_before = a_before * a_k, a_k * b_before + drive[k : k + 1, :]
+        head_a.append(a_before)
+        head_b.append(b_before)
+    runs_a, runs_b = [], []
     for s in range(SUB):
+        runs_a.append(a_before)
+        runs_b.append(b_before)
         a_s = ends[0, s : s + 1, :]
         a_before, b_before = a_before * a_s, a_s * b_before + ends[1, s : s + 1, :]
-        runs_a.append(a_before)
-        runs_b.append(b_before)
     pair = jnp.concatenate([a_before, b_before], axis=0)
     sent_out[...] = jnp.broadcast_to(pair[None], sent_out.shape)
-    runs = jnp.concatenate(runs_a[:SUB] + runs_b[:SUB], axis=0)
-    runs_out[...] = runs
-
-    first = lax.broadcasted_iota(jnp.int32, (SUB, width), 0) == 0
-    times = jnp.where(first, a_head, 1.0)
-    plus = jnp.where(first, b_head, 0.0)
-    rows = 4 * SUB
-    times, plus = (jnp.concatenate([v] * (rows // SUB), axis=0) for v in (times, plus))
-
-    def gate_rows(i, patch=False):
-        at = pl.ds(pl.multiple_of(i * rows, rows), rows)
-        ph, pp, pg = h[at, :], p[at, :], g[at, :]
-        ph, pp = ph + pp * plus, pp * times
-        if patch:
-            r = lax.broadcasted_iota(jnp.int32, (rows, width), 0)
-            for k, (a_k, b_k) in enumerate(opening):
-                ph, pp = jnp.where(r == k * SUB, b_k, ph), jnp.where(r == k * SUB, a_k, pp)
-        gated_h[at, :] = (ph * pg).astype(bf16)
-        gated_p[at, :] = (pp * pg).astype(bf16)
-
-    gate_rows(0, True)
-    lax.fori_loop(1, length // rows, lambda i, _: (gate_rows(i), 0)[1], 0)
-
-    def back(gated, begin):
-        t = lax.broadcasted_iota(jnp.int32, (half, length), 0) + begin
-        c = lax.broadcasted_iota(jnp.int32, (half, length), 1)
-        pick = jnp.where(t == (c & (SUB - 1)) * run + (c >> 3), 1.0, 0.0).astype(bf16)
-        return dot(pick, gated[...]).astype(bf16)
-
-    tp = lax.axis_index("tp")
-    for i, gated in enumerate((gated_h, gated_p)):
-        packed_out[pl.ds(i * half, half), :] = back(gated, (1 - tp) * half)
-        mine_out[pl.ds(i * half, half), :] = back(gated, tp * half)
-    rest = runs
+    small = jnp.concatenate(runs_a + runs_b + head_a + head_b, axis=0)
+    small = jnp.concatenate([small, jnp.zeros((SMALL - small.shape[0], width), f32)], axis=0)
+    small_out[...] = small
     for i in range(PARTS):
-        part = rest.astype(bf16)
-        packed_out[pl.ds((cols + 1) * width + i * 2 * SUB, 2 * SUB), :] = part
-        rest = rest - part.astype(f32)
-    for copy in copies:
-        copy.wait()
+        part = small.astype(bf16)
+        packed_out[pl.ds(packed.shape[0] - (PARTS - i) * SMALL, SMALL), :] = part
+        small = small - part.astype(f32)
 
 
 def before_in(pieces, index):
@@ -307,7 +287,7 @@
         sent_out[k] = jnp.where(k == partner, before, pair)
 
 
-def out_kernel(pieces, before, runs, mine, packed, received, out, theirs, block, gated_mine, gated_theirs, sent):
+def out_kernel(pieces, before, small, mine, packed, received, out, theirs, block, gated_mine, gated_theirs, sent):
     half, width = out.shape[0], mine.shape[1]
     run = half // (SUB // 2)
     deep = pieces.shape[0] // 2
@@ -318,21 +298,25 @@
     own = [jnp.where(is_one, pieces[2 * k + 1], pieces[2 * k]) for k in range(deep)]
     cols = out.shape[1] // width
     last = (cols + 1) * width
-    their_runs = sum(received[pl.ds(last + i * 2 * SUB, 2 * SUB), :].astype(f32) for i in range(PARTS))
+    their_small = sum(received[pl.ds(last + i * SMALL, SMALL), :].astype(f32) for i in range(PARTS))
     sides = (
-        (own, before[...], runs[...], mine, gated_mine),
-        ([theirs[k] for k in range(deep)], theirs[at], their_runs, received, gated_theirs),
-    )
+        (own, before[...], small[...], mine, gated_mine),
+        ([theirs[k] for k in range(deep)], theirs[at], their_small, received, gated_theirs),
+    )
+    row = lax.broadcasted_iota(jnp.int32, (run, width), 0) + tp * half
     for totals, near, steps, parts, gated in sides:
         (_, b_at), _ = before_in(totals, at)
         carried = near[0:1] * b_at + near[1:2]
-        start = steps[:SUB] * carried + steps[SUB:]
+        start = steps[:SUB] * carried + steps[SUB : 2 * SUB]
         start = jnp.where(is_one, start[SUB // 2 :], start[: SUB // 2])
         for u in range(SUB // 2):
             here, there = pl.ds(u * run, run), pl.ds(half + u * run, run)
-            gated[here, :] = (
-                parts[here, :].astype(f32) + parts[there, :].astype(f32) * start[u : u + 1]
-            ).astype(bf16)
+            enter = start[u : u + 1]
+            if u == 0:
+                for k in range(HEADS):
+                    a_k, b_k = steps[2 * SUB + k : 2 * SUB + k + 1], steps[2 * SUB + HEADS + k : 2 * SUB + HEADS + k + 1]
+                    enter = jnp.where(row == k, a_k * carried + b_k, enter)
+            gated[here, :] = (parts[here, :].astype(f32) + parts[there, :].astype(f32) * enter).astype(bf16)
     copies = []
     for q in range(cols):
         w = pl.ds((q + 1) * width, width)
@@ -348,10 +332,12 @@
 
 HBM = pl.BlockSpec(memory_space=pltpu.HBM)
 PARTS = 3
+SMALL = 32
+HEADS = 3
 LATER = 8
 
 
-def call(kernel, inputs, out_shape, scratch=(), out_specs=None):
+def call(kernel, inputs, out_shape, scratch=(), out_specs=None, aliases=None):
     run = pl.pallas_call(
         kernel,
         out_shape=out_shape,
@@ -359,6 +345,7 @@
         scratch_shapes=list(scratch),
         compiler_params=pltpu.CompilerParams(vmem_limit_bytes=32 * 1024 * 1024),
         in_specs=[VMEM] * inputs[0] + [HBM] * inputs[1],
+        input_output_aliases=aliases or {},
     )
 
     def place(i, a):
@@ -421,34 +408,34 @@
     w_gate, conv, w_decay, b_decay, w_input, b_input, rate, offset = held
     halo = lax.ppermute(tail, SP, [(s, s + 1) for s in range(count - 1)])
     taps = conv_weight.shape[0]
-    h, p, g, ends, blocks, shift = call(
+    cols = features // width
+    packed_shape = big(((cols + 1) * width + PARTS * SMALL, width), bf16)
+    half_square = big((length, width), bf16)
+    mine, packed, ends, blocks, shift = call(
         scan_kernel,
-        (11, 0),
+        (11, 1),
         (
-            square, square, square, big((2, SUB, width), f32),
+            half_square, packed_shape, big((2, SUB, width), f32),
             big((heads * block // 256, 256, 512), bf16), big((HALO * SUB, width), f32),
         ),
         scratch=[
-            big((length, width), bf16), square, square, square,
-            big((length + (taps - 1) * SUB, width), f32), big((length, width), bf16),
+            half_square, square, square, square,
+            big((length + (taps - 1) * SUB, width), f32), half_square,
+            square, square, half_square, half_square, pltpu.SemaphoreType.DMA((cols,)),
         ],
-    )(inner, normed_own, normed_other, w_gate, conv, w_decay, b_decay, w_input, b_input, rate, offset)
-    cols = features // width
-    packed_rows = (cols + 1) * width + PARTS * 2 * SUB
-    runs, mine, packed, sent = call(
+    )(
+        inner, normed_own, normed_other, w_gate, conv, w_decay, b_decay, w_input, b_input, rate, offset, out_weight,
+    )
+    small, packed, sent = call(
         pack_kernel,
-        (12, 1),
-        (
-            big((2 * SUB, width), f32), big((length, width), bf16),
-            big((packed_rows, width), bf16), big((plane, 2, width), f32),
-        ),
+        (10, 0),
+        (big((SMALL, width), f32), packed_shape, big((plane, 2, width), f32)),
         scratch=[
             big((2 * HALO, width), f32), big((2 * HALO, width), bf16),
             big((HALO, width), f32), big((HALO, width), f32),
-            big((length, width), bf16), big((length, width), bf16),
-            pltpu.SemaphoreType.DMA((cols,)),
         ],
-    )(inner, halo, conv, blocks, b_decay, b_input, rate, shift, ends, h, p, g, out_weight)
+        aliases={9: 1},
+    )(inner, halo, conv, blocks, b_decay, b_input, rate, shift, ends, packed)
     received = lax.ppermute(packed, "tp", swap)
     pieces = lax.all_to_all(sent, PLANE, split_axis=0, concat_axis=0, tiled=True)
     before, sent = call(plane_kernel, (1, 0), (big((2, width), f32), big((2 * deep, 2, width), f32)))(pieces)
@@ -462,7 +449,7 @@
             big((half, width), bf16), big((half, width), bf16), pltpu.SemaphoreType.DMA((cols,)),
         ),
         out_specs=HBM,
-    )(pieces, before, runs, mine, packed, received)
+    )(pieces, before, small, mine, packed, received)
 
 
 def solution(mesh):

time: 60.1 us -> 59.8 us (level)
  transfers between devices with their start and end apart: 3 -> 3, of which waited for: 0 -> 0; matrix products, arithmetic and copies ran while one was open for 0% -> 0% of each run, Pallas kernels for 12% -> 13%
where the time goes in v5:
time: 59.8 us; the launch traced here: 59.5 us
  blocking collectives  35.2 us (59%)
  Pallas kernels  12.3 us (21%)
  starting transfers between devices  11.9 us (20%)
    all_to_all x1, blocking collectives, step(): lax.all_to_all(sent, ('sp_0', 'tp'), split_axis=0, concat_axis=0, tiled=T...  19.8 us
    all_to_all x1, blocking collectives, step(): lax.all_to_all(sent, PLANE, split_axis=0, concat_axis=0, tiled=True)  15.4 us
    pallas_call x6, Pallas kernels, call(): return lambda *args: run(*(place(i, a) for i, a in enumerate(args)))  12.3 us
    ppermute x1, starting transfers between devices, step(): other = lax.ppermute(tokens, 'tp', swap)  8.73 us
    ppermute x1, starting transfers between devices, step(): received = lax.ppermute(packed, 'tp', swap)  1.92 us
    ppermute x1, starting transfers between devices, step(): halo = lax.ppermute(tail, SP, [(s, s + 1) for s in range(count - 1)])  1.29 us
  transfers between devices with their start and end apart: 3, of which 0 were waited for; matrix products, arithmetic and copies ran while one was open for 0% of the time, Pallas kernels for 13%

profile of v5, /device:TPU:1, one launch (start us, length us, event | category | flops | bytes accessed | tf_op | source)
XLA Modules:
  0.0 59.5 jit_solution(17576291253051008159)
XLA Ops:
  0.0 8.7 %collective-permute-start = (bf16[256,2048]{1,0:T(8,128)(2,1)}, bf16[256,2048]{1,0:T(8,128)(2,1)S(1)}, u32[]{:S(2)}, u32[]{:S(2)}) collective-permute-start(bf16[256,2048]{1,0:T(8,128)(2,1)} %own_in.1), channel_id=1, source_target_pairs={{0,1},{1,0},{2,3},{3,2},{4,5},{5,4},{6,7},{7,6},{8,9},{9,8},{10,11... | collective-permute-start | bytes 3145736 | tf_op jit(solution)/shard_map/ppermute | solution.py:381
  8.7 3.1 %shard_map.118 = (bf16[256,512]{1,0:T(8,128)(2,1)S(1)}, bf16[256,2048]{1,0:T(8,128)(2,1)S(1)}, f32[1,2048]{1,0:T(1,128)S(1)}, bf16[2048,512]{1,0:T(8,128)(2,1)S(1)}) custom-call(f32[1,2048]{1,0:T(1,128)} %bitcast.4, bf16[2048,512]{1,0:T(8,128)(2,1)} %w_in_in.1, bf16[256,2048]{1,0:T(8,128)(2,1)} %own_in.1), custom_call_target="tpu_custom_call" | custom-call | tf_op jit(solution)/shard_map/pallas_call | solution.py:354
  11.9 0.0 collective-permute-done.other
  11.9 2.0 %shard_map.119 = (bf16[512,512]{1,0:T(8,128)(2,1)S(1)}, bf16[8,512]{1,0:T(8,128)(2,1)S(1)}, bf16[256,2048]{1,0:T(8,128)(2,1)S(1)}, bf16[2048,512]{1,0:T(8,128)(2...) custom-call(bf16[256,2048]{1,0:T(8,128)(2,1)S(1)} %collective-permut, ...), custom_call_target="tpu_custom_call" | custom-call | tf_op jit(solution)/shard_map/pallas_call | solution.py:354
  13.9 1.3 %collective-permute-start.1 = (bf16[8,512]{1,0:T(8,128)(2,1)S(1)}, bf16[8,512]{1,0:T(8,128)(2,1)S(1)}, u32[]{:S(2)}, u32[]{:S(2)}) collective-permute-start(bf16[8,512]{1,0:T(8,128)(2,1)S(1)} %get-tuple-element.34), channel_id=1, source_target_pairs={{0,2},{2,4},{4,6},{6,8},{8,10},{10,12},{12,14},{14,16},{16,18},{18... | collective-permute-start | bytes 24584 | tf_op jit(solution)/shard_map/ppermute | solution.py:409
  15.2 4.8 %shard_map.120 = (bf16[512,512]{1,0:T(8,128)(2,1)S(1)}, bf16[2656,512]{1,0:T(8,128)(2,1)S(1)}, f32[2,8,512]{2,1,0:T(8,128)S(1)}, bf16[2,256,512]{2,1,0:T(8,128)(2,1)S(1)}, f32[64,512]{1,0:T(8,128)S(1)}) custom-call(bf16[512,512]{1,0:T(8,128)(2,1)S(1)} %get-tuple-element.33.inner, bf16[256,2048]{1,0:T(8,128)(2,1)S(1)} %get-tuple-element.36.normed_own, ...), custom_call_target="tpu_custom_call" | custom-call | tf_op jit(solution)/shard_map/pallas_call | solution.py:354
  19.9 0.0 collective-permute-done.1.halo
  19.9 0.3 shard_map.121
  20.2 1.9 %collective-permute-start.2 = (bf16[2656,512]{1,0:T(8,128)(2,1)S(1)}, bf16[2656,512]{1,0:T(8,128)(2,1)S(1)}, u32[]{:S(2)}, u32[]{:S(2)}) collective-permute-start(bf16[2656,512]{1,0:T(8,128)(2,1)S(1)} %get-tuple-element.54.packed), channel_id=1, source_target_pairs={{0,1},{1,0},{2,3},{3,2},{4,5},{5,4},{6,7},{7,6},{8,9},{9,8},{10,11... | collective-permute-start | bytes 8159240 | tf_op jit(solution)/shard_map/ppermute | solution.py:439
  22.1 15.4 %all_to_all.10.pieces = f32[32,2,512]{2,1,0:T(2,128)S(1)} all-to-all(f32[32,2,512]{2,1,0:T(2,128)S(1)} %get-tuple-element.49), channel_id=1, replica_groups=mesh['sp_0'=8,'sp_1'=8,'sp_2'=4,'tp'=2] {'sp_1','sp_2'}, dimensions={0} | all-to-all | bytes 262144 | tf_op jit(solution)/shard_map/all_to_all | solution.py:440
  37.5 0.1 shard_map.122
  37.6 19.8 %all_to_all.11.pieces = f32[16,2,512]{2,1,0:T(2,128)S(1)} all-to-all(f32[16,2,512]{2,1,0:T(2,128)S(1)} %get-tuple-element.50), channel_id=1, replica_groups=mesh['sp_0'=8,'sp_1'=8,'sp_2'=4,'tp'=2] {'sp_0','tp'}, dimensions={0} | all-to-all | bytes 131072 | tf_op jit(solution)/shard_map/all_to_all | solution.py:442
  57.5 0.0 collective-permute-done.2.received
  57.5 2.1 %shard_map.123 = bf16[256,2048]{1,0:T(8,128)(2,1)} custom-call(f32[16,2,512]{2,1,0:T(2,128)S(1)} %all_to_all.11.pieces, f32[2,512]{1,0:T(2,128)S(1)} %get-tuple-element.51.before, f32[32,512]{1,0:T(8,128)S(1)} %get-tuple-element.52.small, bf16[512,512]{1,0:T(8,128)(2,1)S(1)} %get-tuple-element.53.mine, bf16[2656,512]{1,0:T(8,128)(2,1)S(1)} %get-tuple-element.54.packed, ...), custom_call_target="tpu_custom_call" | custom-call | tf_op jit(solution)/shard_map/pallas_call | solution.py:354
Async XLA Ops:
  0.0 11.9 %collective-permute-start = (bf16[256,2048]{1,0:T(8,128)(2,1)}, bf16[256,2048]{1,0:T(8,128)(2,1)S(1)}, u32[]{:S(2)}, u32[]{:S(2)}) collective-permute-start(bf16[256,2048]{1,0:T(8,128)(2,1)} %own_in.1), channel_id=1, source_target_pairs={{0,1},{1,0},{2,3},{3,2},{4,5},{5,4},{6,7},{7,6},{8,9},{9,8},{10,11... | collective-permute-start | bytes 3145736 | tf_op jit(solution)/shard_map/ppermute | solution.py:381
  13.9 6.1 %collective-permute-start.1 = (bf16[8,512]{1,0:T(8,128)(2,1)S(1)}, bf16[8,512]{1,0:T(8,128)(2,1)S(1)}, u32[]{:S(2)}, u32[]{:S(2)}) collective-permute-start(bf16[8,512]{1,0:T(8,128)(2,1)S(1)} %get-tuple-element.34), channel_id=1, source_target_pairs={{0,2},{2,4},{4,6},{6,8},{8,10},{10,12},{12,14},{14,16},{16,18},{18... | collective-permute-start | bytes 24584 | tf_op jit(solution)/shard_map/ppermute | solution.py:409
  20.2 37.3 %collective-permute-start.2 = (bf16[2656,512]{1,0:T(8,128)(2,1)S(1)}, bf16[2656,512]{1,0:T(8,128)(2,1)S(1)}, u32[]{:S(2)}, u32[]{:S(2)}) collective-permute-start(bf16[2656,512]{1,0:T(8,128)(2,1)S(1)} %get-tuple-element.54.packed), channel_id=1, source_target_pairs={{0,1},{1,0},{2,3},{3,2},{4,5},{5,4},{6,7},{7,6},{8,9},{9,8},{10,11... | collective-permute-start | bytes 8159240 | tf_op jit(solution)/shard_map/ppermute | solution.py:439

commit v6 on v5

--- a/solution.py
+++ b/solution.py
@@ -7,7 +7,7 @@
 from jax.sharding import PartitionSpec as P
 
 SP = ("sp_0", "sp_1", "sp_2")
-PLANE = ("sp_1", "sp_2")
+PLANE = ("sp_2", "sp_1")
 SP_TP = ("sp_0", "sp_1", "sp_2", "tp")
 
 EPSILON = 1e-05
@@ -20,19 +20,19 @@
     return jnp.dot(a, b, preferred_element_type=f32)
 
 
-def norm_tokens(source, target, gain, middle, scale, ready=None):
+def norm_tokens(source, target, gain, middle, scale, ready=None, arrivals=()):
     half, features = source.shape
     step, lanes = 32, 128
 
     def tiles(r):
         return [source[r, t : t + lanes].astype(f32) for t in range(0, features, lanes)]
 
-    def by_rows(one):
+    def by_rows(one, first=0, last=half // step):
         def rows(i, _):
             one(pl.ds(pl.multiple_of(i * step, step), step))
             return 0
 
-        lax.fori_loop(0, half // step, rows, 0)
+        lax.fori_loop(first, last, rows, 0)
 
     def over_features(stat):
         return jnp.broadcast_to(jnp.sum(stat[...], axis=1, keepdims=True) * (1.0 / features), stat.shape)
@@ -40,7 +40,11 @@
     def add_up(r):
         middle[r, :] = sum(tiles(r))
 
-    by_rows(add_up)
+    each = half // step // max(1, len(arrivals))
+    for i, arrival in enumerate(arrivals or (None,)):
+        if arrival is not None:
+            arrival.wait()
+        by_rows(add_up, i * each, (i + 1) * each)
     middle[...] = over_features(middle)
 
     def add_squares(r):
@@ -68,9 +72,12 @@
 
 
 def own_tokens_kernel(gain_in, w_in_in, own_in, inner, normed, gain, w_in, own, arrived, middle, scale):
-    copies = fetch((gain_in, w_in_in, own_in), (gain, w_in, own), arrived, (2, 0, 1))
-    copies[2].wait()
-    norm_tokens(own, normed, gain, middle, scale, copies[0])
+    rows = own.shape[0] // 2
+    halves = [pl.ds(i * rows, rows) for i in range(2)]
+    copies = fetch(
+        (gain_in, w_in_in, *(own_in.at[r] for r in halves)), (gain, w_in, *(own.at[r] for r in halves)), arrived, (2, 3, 0, 1)
+    )
+    norm_tokens(own, normed, gain, middle, scale, copies[0], copies[2:])
     copies[1].wait()
     inner[...] = dot(normed[...], w_in[...]).astype(bf16)
 
@@ -278,11 +285,13 @@
 
 def plane_kernel(pieces, before_out, sent_out):
     index = lax.axis_index("sp_1") * lax.axis_size("sp_2") + lax.axis_index("sp_2")
-    (a_at, b_at), (a, b) = before_in([pieces[k] for k in range(pieces.shape[0])], index)
+    wide, high = lax.axis_size("sp_2"), lax.axis_size("sp_1")
+    in_order = [pieces[k % wide * high + k // wide] for k in range(pieces.shape[0])]
+    (a_at, b_at), (a, b) = before_in(in_order, index)
     before = jnp.concatenate([a_at, b_at], axis=0)
     before_out[...] = before
     pair = jnp.concatenate([a, b], axis=0)
-    partner = lax.axis_index("sp_0") * 2 + 1 - lax.axis_index("tp")
+    partner = (1 - lax.axis_index("tp")) * lax.axis_size("sp_0") + lax.axis_index("sp_0")
     for k in range(sent_out.shape[0]):
         sent_out[k] = jnp.where(k == partner, before, pair)
 
@@ -294,8 +303,8 @@
     at, tp = lax.axis_index("sp_0"), lax.axis_index("tp")
     is_one = tp == 1
     for k in range(deep):
-        theirs[k] = jnp.where(is_one, pieces[2 * k], pieces[2 * k + 1])
-    own = [jnp.where(is_one, pieces[2 * k + 1], pieces[2 * k]) for k in range(deep)]
+        theirs[k] = jnp.where(is_one, pieces[k], pieces[deep + k])
+    own = [jnp.where(is_one, pieces[deep + k], pieces[k]) for k in range(deep)]
     cols = out.shape[1] // width
     last = (cols + 1) * width
     their_small = sum(received[pl.ds(last + i * SMALL, SMALL), :].astype(f32) for i in range(PARTS))
@@ -318,11 +327,14 @@
                     enter = jnp.where(row == k, a_k * carried + b_k, enter)
             gated[here, :] = (parts[here, :].astype(f32) + parts[there, :].astype(f32) * enter).astype(bf16)
     copies = []
+    narrow = block.shape[2]
     for q in range(cols):
         w = pl.ds((q + 1) * width, width)
-        block[q] = (dot(gated_mine[...], packed[w, :]) + dot(gated_theirs[...], received[w, :])).astype(bf16)
-        copies.append(pltpu.make_async_copy(block.at[q], out.at[:, pl.ds(q * width, width)], sent.at[q]))
-        copies[q].start()
+        for i in range(width // narrow):
+            part, k = pl.ds(i * narrow, narrow), q * (width // narrow) + i
+            block[k] = (dot(gated_mine[...], packed[w, part]) + dot(gated_theirs[...], received[w, part])).astype(bf16)
+            copies.append(pltpu.make_async_copy(block.at[k], out.at[:, pl.ds(k * narrow, narrow)], sent.at[k]))
+            copies[k].start()
     for copy in copies:
         copy.wait()
 
@@ -394,7 +406,7 @@
         own_tokens_kernel,
         (0, 3),
         (big((half, width), bf16), big((half, features), bf16), like(gain), like(in_weight)),
-        scratch=[like(tokens), pltpu.SemaphoreType.DMA((3,)), *stats],
+        scratch=[like(tokens), pltpu.SemaphoreType.DMA((4,)), *stats],
     )(gain, in_weight, tokens)
     inner, tail, normed_other, *held = call(
         other_tokens_kernel,
@@ -439,7 +451,7 @@
     received = lax.ppermute(packed, "tp", swap)
     pieces = lax.all_to_all(sent, PLANE, split_axis=0, concat_axis=0, tiled=True)
     before, sent = call(plane_kernel, (1, 0), (big((2, width), f32), big((2 * deep, 2, width), f32)))(pieces)
-    pieces = lax.all_to_all(sent, ("sp_0", "tp"), split_axis=0, concat_axis=0, tiled=True)
+    pieces = lax.all_to_all(sent, ("tp", "sp_0"), split_axis=0, concat_axis=0, tiled=True)
     return call(
         out_kernel,
         (6, 0),

time: 59.8 us -> 58.9 us (0.985)
  blocking collectives: 35.2 us -> 34.4 us
where the time goes in v6:
time: 58.9 us; the launch traced here: 58.6 us
  blocking collectives  34.4 us (58%)
  Pallas kernels  12.2 us (21%)
  starting transfers between devices  11.9 us (20%)
    all_to_all x1, blocking collectives, step(): lax.all_to_all(sent, ('tp', 'sp_0'), split_axis=0, concat_axis=0, tiled=T...  19.4 us
    all_to_all x1, blocking collectives, step(): lax.all_to_all(sent, PLANE, split_axis=0, concat_axis=0, tiled=True)  15.1 us
    pallas_call x6, Pallas kernels, call(): return lambda *args: run(*(place(i, a) for i, a in enumerate(args)))  12.2 us
    ppermute x1, starting transfers between devices, step(): other = lax.ppermute(tokens, 'tp', swap)  8.73 us
    ppermute x1, starting transfers between devices, step(): received = lax.ppermute(packed, 'tp', swap)  1.92 us
    ppermute x1, starting transfers between devices, step(): halo = lax.ppermute(tail, SP, [(s, s + 1) for s in range(count - 1)])  1.29 us
  transfers between devices with their start and end apart: 3, of which 0 were waited for; matrix products, arithmetic and copies ran while one was open for 0% of the time, Pallas kernels for 13%

profile of v6, /device:TPU:1, one launch (start us, length us, event | category | flops | bytes accessed | tf_op | source)
XLA Modules:
  0.0 58.6 jit_solution(8124810171002047548)
XLA Ops:
  0.0 8.7 %collective-permute-start = (bf16[256,2048]{1,0:T(8,128)(2,1)}, bf16[256,2048]{1,0:T(8,128)(2,1)S(1)}, u32[]{:S(2)}, u32[]{:S(2)}) collective-permute-start(bf16[256,2048]{1,0:T(8,128)(2,1)} %own_in.1), channel_id=1, source_target_pairs={{0,1},{1,0},{2,3},{3,2},{4,5},{5,4},{6,7},{7,6},{8,9},{9,8},{10,11... | collective-permute-start | bytes 3145736 | tf_op jit(solution)/shard_map/ppermute | solution.py:393
  8.7 3.0 %shard_map.118 = (bf16[256,512]{1,0:T(8,128)(2,1)S(1)}, bf16[256,2048]{1,0:T(8,128)(2,1)S(1)}, f32[1,2048]{1,0:T(1,128)S(1)}, bf16[2048,512]{1,0:T(8,128)(2,1)S(1)}) custom-call(f32[1,2048]{1,0:T(1,128)} %bitcast.4, bf16[2048,512]{1,0:T(8,128)(2,1)} %w_in_in.1, bf16[256,2048]{1,0:T(8,128)(2,1)} %own_in.1), custom_call_target="tpu_custom_call" | custom-call | tf_op jit(solution)/shard_map/pallas_call | solution.py:366
  11.7 0.0 collective-permute-done.other
  11.7 2.0 %shard_map.119 = (bf16[512,512]{1,0:T(8,128)(2,1)S(1)}, bf16[8,512]{1,0:T(8,128)(2,1)S(1)}, bf16[256,2048]{1,0:T(8,128)(2,1)S(1)}, bf16[2048,512]{1,0:T(8,128)(2...) custom-call(bf16[256,2048]{1,0:T(8,128)(2,1)S(1)} %collective-permut, ...), custom_call_target="tpu_custom_call" | custom-call | tf_op jit(solution)/shard_map/pallas_call | solution.py:366
  13.8 1.3 %collective-permute-start.1 = (bf16[8,512]{1,0:T(8,128)(2,1)S(1)}, bf16[8,512]{1,0:T(8,128)(2,1)S(1)}, u32[]{:S(2)}, u32[]{:S(2)}) collective-permute-start(bf16[8,512]{1,0:T(8,128)(2,1)S(1)} %get-tuple-element.34), channel_id=1, source_target_pairs={{0,2},{2,4},{4,6},{6,8},{8,10},{10,12},{12,14},{14,16},{16,18},{18... | collective-permute-start | bytes 24584 | tf_op jit(solution)/shard_map/ppermute | solution.py:421
  15.0 4.8 %shard_map.120 = (bf16[512,512]{1,0:T(8,128)(2,1)S(1)}, bf16[2656,512]{1,0:T(8,128)(2,1)S(1)}, f32[2,8,512]{2,1,0:T(8,128)S(1)}, bf16[2,256,512]{2,1,0:T(8,128)(2,1)S(1)}, f32[64,512]{1,0:T(8,128)S(1)}) custom-call(bf16[512,512]{1,0:T(8,128)(2,1)S(1)} %get-tuple-element.33.inner, bf16[256,2048]{1,0:T(8,128)(2,1)S(1)} %get-tuple-element.36.normed_own, ...), custom_call_target="tpu_custom_call" | custom-call | tf_op jit(solution)/shard_map/pallas_call | solution.py:366
  19.8 0.0 collective-permute-done.1.halo
  19.8 0.3 shard_map.121
  20.1 1.9 %collective-permute-start.2 = (bf16[2656,512]{1,0:T(8,128)(2,1)S(1)}, bf16[2656,512]{1,0:T(8,128)(2,1)S(1)}, u32[]{:S(2)}, u32[]{:S(2)}) collective-permute-start(bf16[2656,512]{1,0:T(8,128)(2,1)S(1)} %get-tuple-element.54.packed), channel_id=1, source_target_pairs={{0,1},{1,0},{2,3},{3,2},{4,5},{5,4},{6,7},{7,6},{8,9},{9,8},{10,11... | collective-permute-start | bytes 8159240 | tf_op jit(solution)/shard_map/ppermute | solution.py:451
  22.0 15.1 %all_to_all.10.pieces = f32[32,2,512]{2,1,0:T(2,128)S(1)} all-to-all(f32[32,2,512]{2,1,0:T(2,128)S(1)} %get-tuple-element.49), channel_id=1, replica_groups=mesh['sp_0'=8,'sp_1'=8,'sp_2'=4,'tp'=2] {'sp_2','sp_1'}, dimensions={0} | all-to-all | bytes 262144 | tf_op jit(solution)/shard_map/all_to_all | solution.py:452
  37.1 0.1 shard_map.122
  37.2 19.4 %all_to_all.11.pieces = f32[16,2,512]{2,1,0:T(2,128)S(1)} all-to-all(f32[16,2,512]{2,1,0:T(2,128)S(1)} %get-tuple-element.50), channel_id=1, replica_groups=mesh['sp_0'=8,'sp_1'=8,'sp_2'=4,'tp'=2] {'tp','sp_0'}, dimensions={0} | all-to-all | bytes 131072 | tf_op jit(solution)/shard_map/all_to_all | solution.py:454
  56.6 0.0 collective-permute-done.2.received
  56.6 2.1 %shard_map.123 = bf16[256,2048]{1,0:T(8,128)(2,1)} custom-call(f32[16,2,512]{2,1,0:T(2,128)S(1)} %all_to_all.11.pieces, f32[2,512]{1,0:T(2,128)S(1)} %get-tuple-element.51.before, f32[32,512]{1,0:T(8,128)S(1)} %get-tuple-element.52.small, bf16[512,512]{1,0:T(8,128)(2,1)S(1)} %get-tuple-element.53.mine, bf16[2656,512]{1,0:T(8,128)(2,1)S(1)} %get-tuple-element.54.packed, ...), custom_call_target="tpu_custom_call" | custom-call | tf_op jit(solution)/shard_map/pallas_call | solution.py:366
Async XLA Ops:
  0.0 11.7 %collective-permute-start = (bf16[256,2048]{1,0:T(8,128)(2,1)}, bf16[256,2048]{1,0:T(8,128)(2,1)S(1)}, u32[]{:S(2)}, u32[]{:S(2)}) collective-permute-start(bf16[256,2048]{1,0:T(8,128)(2,1)} %own_in.1), channel_id=1, source_target_pairs={{0,1},{1,0},{2,3},{3,2},{4,5},{5,4},{6,7},{7,6},{8,9},{9,8},{10,11... | collective-permute-start | bytes 3145736 | tf_op jit(solution)/shard_map/ppermute | solution.py:393
  13.8 6.1 %collective-permute-start.1 = (bf16[8,512]{1,0:T(8,128)(2,1)S(1)}, bf16[8,512]{1,0:T(8,128)(2,1)S(1)}, u32[]{:S(2)}, u32[]{:S(2)}) collective-permute-start(bf16[8,512]{1,0:T(8,128)(2,1)S(1)} %get-tuple-element.34), channel_id=1, source_target_pairs={{0,2},{2,4},{4,6},{6,8},{8,10},{10,12},{12,14},{14,16},{16,18},{18... | collective-permute-start | bytes 24584 | tf_op jit(solution)/shard_map/ppermute | solution.py:421
  20.1 36.5 %collective-permute-start.2 = (bf16[2656,512]{1,0:T(8,128)(2,1)S(1)}, bf16[2656,512]{1,0:T(8,128)(2,1)S(1)}, u32[]{:S(2)}, u32[]{:S(2)}) collective-permute-start(bf16[2656,512]{1,0:T(8,128)(2,1)S(1)} %get-tuple-element.54.packed), channel_id=1, source_target_pairs={{0,1},{1,0},{2,3},{3,2},{4,5},{5,4},{6,7},{7,6},{8,9},{9,8},{10,11... | collective-permute-start | bytes 8159240 | tf_op jit(solution)/shard_map/ppermute | solution.py:451

commit v7 on v6

--- a/solution.py
+++ b/solution.py
@@ -291,7 +291,7 @@
     before = jnp.concatenate([a_at, b_at], axis=0)
     before_out[...] = before
     pair = jnp.concatenate([a, b], axis=0)
-    partner = (1 - lax.axis_index("tp")) * lax.axis_size("sp_0") + lax.axis_index("sp_0")
+    partner = lax.axis_index("sp_0") * 2 + 1 - lax.axis_index("tp")
     for k in range(sent_out.shape[0]):
         sent_out[k] = jnp.where(k == partner, before, pair)
 
@@ -303,8 +303,8 @@
     at, tp = lax.axis_index("sp_0"), lax.axis_index("tp")
     is_one = tp == 1
     for k in range(deep):
-        theirs[k] = jnp.where(is_one, pieces[k], pieces[deep + k])
-    own = [jnp.where(is_one, pieces[deep + k], pieces[k]) for k in range(deep)]
+        theirs[k] = jnp.where(is_one, pieces[2 * k], pieces[2 * k + 1])
+    own = [jnp.where(is_one, pieces[2 * k + 1], pieces[2 * k]) for k in range(deep)]
     cols = out.shape[1] // width
     last = (cols + 1) * width
     their_small = sum(received[pl.ds(last + i * SMALL, SMALL), :].astype(f32) for i in range(PARTS))
@@ -451,7 +451,7 @@
     received = lax.ppermute(packed, "tp", swap)
     pieces = lax.all_to_all(sent, PLANE, split_axis=0, concat_axis=0, tiled=True)
     before, sent = call(plane_kernel, (1, 0), (big((2, width), f32), big((2 * deep, 2, width), f32)))(pieces)
-    pieces = lax.all_to_all(sent, ("tp", "sp_0"), split_axis=0, concat_axis=0, tiled=True)
+    pieces = lax.all_to_all(sent, ("sp_0", "tp"), split_axis=0, concat_axis=0, tiled=True)
     return call(
         out_kernel,
         (6, 0),

time: 58.9 us -> 59.5 us (1.010)
  blocking collectives: 34.4 us -> 35.1 us
    all_to_all x1, blocking collectives: 19.4 us -> 20 us  [step(): lax.all_to_all(sent, ('sp_0', 'tp'), split_axis=0, concat_axis=0, tiled=T...]
where the time goes in v7:
time: 59.5 us; the launch traced here: 59.3 us
  blocking collectives  35.1 us (59%)
  Pallas kernels  12.2 us (21%)
  starting transfers between devices  11.9 us (20%)
    all_to_all x1, blocking collectives, step(): lax.all_to_all(sent, ('sp_0', 'tp'), split_axis=0, concat_axis=0, tiled=T...  20 us
    all_to_all x1, blocking collectives, step(): lax.all_to_all(sent, PLANE, split_axis=0, concat_axis=0, tiled=True)  15.1 us
    pallas_call x6, Pallas kernels, call(): return lambda *args: run(*(place(i, a) for i, a in enumerate(args)))  12.2 us
    ppermute x1, starting transfers between devices, step(): other = lax.ppermute(tokens, 'tp', swap)  8.73 us
    ppermute x1, starting transfers between devices, step(): received = lax.ppermute(packed, 'tp', swap)  1.92 us
    ppermute x1, starting transfers between devices, step(): halo = lax.ppermute(tail, SP, [(s, s + 1) for s in range(count - 1)])  1.29 us
  transfers between devices with their start and end apart: 3, of which 0 were waited for; matrix products, arithmetic and copies ran while one was open for 0% of the time, Pallas kernels for 13%

profile of v7, /device:TPU:1, one launch (start us, length us, event | category | flops | bytes accessed | tf_op | source)
XLA Modules:
  0.0 59.3 jit_solution(904668263528100189)
XLA Ops:
  0.0 8.7 %collective-permute-start = (bf16[256,2048]{1,0:T(8,128)(2,1)}, bf16[256,2048]{1,0:T(8,128)(2,1)S(1)}, u32[]{:S(2)}, u32[]{:S(2)}) collective-permute-start(bf16[256,2048]{1,0:T(8,128)(2,1)} %own_in.1), channel_id=1, source_target_pairs={{0,1},{1,0},{2,3},{3,2},{4,5},{5,4},{6,7},{7,6},{8,9},{9,8},{10,11... | collective-permute-start | bytes 3145736 | tf_op jit(solution)/shard_map/ppermute | solution.py:393
  8.7 3.0 %shard_map.118 = (bf16[256,512]{1,0:T(8,128)(2,1)S(1)}, bf16[256,2048]{1,0:T(8,128)(2,1)S(1)}, f32[1,2048]{1,0:T(1,128)S(1)}, bf16[2048,512]{1,0:T(8,128)(2,1)S(1)}) custom-call(f32[1,2048]{1,0:T(1,128)} %bitcast.4, bf16[2048,512]{1,0:T(8,128)(2,1)} %w_in_in.1, bf16[256,2048]{1,0:T(8,128)(2,1)} %own_in.1), custom_call_target="tpu_custom_call" | custom-call | tf_op jit(solution)/shard_map/pallas_call | solution.py:366
  11.7 0.0 collective-permute-done.other
  11.7 2.0 %shard_map.119 = (bf16[512,512]{1,0:T(8,128)(2,1)S(1)}, bf16[8,512]{1,0:T(8,128)(2,1)S(1)}, bf16[256,2048]{1,0:T(8,128)(2,1)S(1)}, bf16[2048,512]{1,0:T(8,128)(2...) custom-call(bf16[256,2048]{1,0:T(8,128)(2,1)S(1)} %collective-permut, ...), custom_call_target="tpu_custom_call" | custom-call | tf_op jit(solution)/shard_map/pallas_call | solution.py:366
  13.8 1.3 %collective-permute-start.1 = (bf16[8,512]{1,0:T(8,128)(2,1)S(1)}, bf16[8,512]{1,0:T(8,128)(2,1)S(1)}, u32[]{:S(2)}, u32[]{:S(2)}) collective-permute-start(bf16[8,512]{1,0:T(8,128)(2,1)S(1)} %get-tuple-element.34), channel_id=1, source_target_pairs={{0,2},{2,4},{4,6},{6,8},{8,10},{10,12},{12,14},{14,16},{16,18},{18... | collective-permute-start | bytes 24584 | tf_op jit(solution)/shard_map/ppermute | solution.py:421
  15.0 4.8 %shard_map.120 = (bf16[512,512]{1,0:T(8,128)(2,1)S(1)}, bf16[2656,512]{1,0:T(8,128)(2,1)S(1)}, f32[2,8,512]{2,1,0:T(8,128)S(1)}, bf16[2,256,512]{2,1,0:T(8,128)(2,1)S(1)}, f32[64,512]{1,0:T(8,128)S(1)}) custom-call(bf16[512,512]{1,0:T(8,128)(2,1)S(1)} %get-tuple-element.33.inner, bf16[256,2048]{1,0:T(8,128)(2,1)S(1)} %get-tuple-element.36.normed_own, ...), custom_call_target="tpu_custom_call" | custom-call | tf_op jit(solution)/shard_map/pallas_call | solution.py:366
  19.8 0.0 collective-permute-done.1.halo
  19.8 0.3 shard_map.121
  20.1 1.9 %collective-permute-start.2 = (bf16[2656,512]{1,0:T(8,128)(2,1)S(1)}, bf16[2656,512]{1,0:T(8,128)(2,1)S(1)}, u32[]{:S(2)}, u32[]{:S(2)}) collective-permute-start(bf16[2656,512]{1,0:T(8,128)(2,1)S(1)} %get-tuple-element.54.packed), channel_id=1, source_target_pairs={{0,1},{1,0},{2,3},{3,2},{4,5},{5,4},{6,7},{7,6},{8,9},{9,8},{10,11... | collective-permute-start | bytes 8159240 | tf_op jit(solution)/shard_map/ppermute | solution.py:451
  22.0 15.1 %all_to_all.10.pieces = f32[32,2,512]{2,1,0:T(2,128)S(1)} all-to-all(f32[32,2,512]{2,1,0:T(2,128)S(1)} %get-tuple-element.49), channel_id=1, replica_groups=mesh['sp_0'=8,'sp_1'=8,'sp_2'=4,'tp'=2] {'sp_2','sp_1'}, dimensions={0} | all-to-all | bytes 262144 | tf_op jit(solution)/shard_map/all_to_all | solution.py:452
  37.1 0.1 shard_map.122
  37.2 20.0 %all_to_all.11.pieces = f32[16,2,512]{2,1,0:T(2,128)S(1)} all-to-all(f32[16,2,512]{2,1,0:T(2,128)S(1)} %get-tuple-element.50), channel_id=1, replica_groups=mesh['sp_0'=8,'sp_1'=8,'sp_2'=4,'tp'=2] {'sp_0','tp'}, dimensions={0} | all-to-all | bytes 131072 | tf_op jit(solution)/shard_map/all_to_all | solution.py:454
  57.2 0.0 collective-permute-done.2.received
  57.2 2.1 %shard_map.123 = bf16[256,2048]{1,0:T(8,128)(2,1)} custom-call(f32[16,2,512]{2,1,0:T(2,128)S(1)} %all_to_all.11.pieces, f32[2,512]{1,0:T(2,128)S(1)} %get-tuple-element.51.before, f32[32,512]{1,0:T(8,128)S(1)} %get-tuple-element.52.small, bf16[512,512]{1,0:T(8,128)(2,1)S(1)} %get-tuple-element.53.mine, bf16[2656,512]{1,0:T(8,128)(2,1)S(1)} %get-tuple-element.54.packed, ...), custom_call_target="tpu_custom_call" | custom-call | tf_op jit(solution)/shard_map/pallas_call | solution.py:366
Async XLA Ops:
  0.0 11.7 %collective-permute-start = (bf16[256,2048]{1,0:T(8,128)(2,1)}, bf16[256,2048]{1,0:T(8,128)(2,1)S(1)}, u32[]{:S(2)}, u32[]{:S(2)}) collective-permute-start(bf16[256,2048]{1,0:T(8,128)(2,1)} %own_in.1), channel_id=1, source_target_pairs={{0,1},{1,0},{2,3},{3,2},{4,5},{5,4},{6,7},{7,6},{8,9},{9,8},{10,11... | collective-permute-start | bytes 3145736 | tf_op jit(solution)/shard_map/ppermute | solution.py:393
  13.8 6.1 %collective-permute-start.1 = (bf16[8,512]{1,0:T(8,128)(2,1)S(1)}, bf16[8,512]{1,0:T(8,128)(2,1)S(1)}, u32[]{:S(2)}, u32[]{:S(2)}) collective-permute-start(bf16[8,512]{1,0:T(8,128)(2,1)S(1)} %get-tuple-element.34), channel_id=1, source_target_pairs={{0,2},{2,4},{4,6},{6,8},{8,10},{10,12},{12,14},{14,16},{16,18},{18... | collective-permute-start | bytes 24584 | tf_op jit(solution)/shard_map/ppermute | solution.py:421
  20.1 37.1 %collective-permute-start.2 = (bf16[2656,512]{1,0:T(8,128)(2,1)S(1)}, bf16[2656,512]{1,0:T(8,128)(2,1)S(1)}, u32[]{:S(2)}, u32[]{:S(2)}) collective-permute-start(bf16[2656,512]{1,0:T(8,128)(2,1)S(1)} %get-tuple-element.54.packed), channel_id=1, source_target_pairs={{0,1},{1,0},{2,3},{3,2},{4,5},{5,4},{6,7},{7,6},{8,9},{9,8},{10,11... | collective-permute-start | bytes 8159240 | tf_op jit(solution)/shard_map/ppermute | solution.py:451
